TPU v7x, 256 devices: a 4x2x16 block of a 4x16x16 slice. The times are simulated.
256 devices in a mesh: grp: 2 (over y), sp: 16 (over z), tp: 8 (over x, core).
Axes of the slice: x: 4, y: 2, z: 16, core: 2. Of those that a mesh axis runs over, the one named last changes fastest.
The devices are a block of a 4x16x16 slice.
Arguments:
- tokens_in: bfloat16 [12288, 4096], P(('grp', 'sp')), parts along dimension 0, may hold values from -6 to 6
- norm_gain: float32 [4096], replicated, may hold values from 0.1 to 1.9
- window_query: bfloat16 [4096, 1024], P('sp', 'tp'), may hold values from -0.09375 to 0.09375
- window_key: bfloat16 [4096, 512], P('sp', 'tp'), may hold values from -0.09375 to 0.09375
- window_value: bfloat16 [4096, 512], P('sp', 'tp'), may hold values from -0.09375 to 0.09375
- window_query_gain: float32 [64], replicated, may hold values from 0.6 to 16
- window_key_gain: float32 [64], replicated, may hold values from 0.6 to 16
- sink_logit: float32 [16], P('tp'), may hold values from 1 to 6
- dense_query: bfloat16 [4096, 1024], P('sp', 'tp'), may hold values from -0.09375 to 0.09375
- dense_key: bfloat16 [4096, 512], P('sp', 'tp'), may hold values from -0.09375 to 0.09375
- dense_value: bfloat16 [4096, 512], P('sp', 'tp'), may hold values from -0.09375 to 0.09375
- dense_query_gain: float32 [64], replicated, may hold values from 1 to 14
- dense_key_gain: float32 [64], replicated, may hold values from 1 to 14
- window_out: bfloat16 [1024, 4096], P('tp', 'sp'), may hold values from -1.5 to 1.5
- dense_out: bfloat16 [1024, 4096], P('tp', 'sp'), may hold values from -3 to 3
Outputs:
- mixed_out: bfloat16 [12288, 4096], P(('grp', 'sp', 'tp')), parts along dimension 0
There are 2 independent parts, one for each index of `grp`. A program takes and returns all parts, laid end to end along the dimension named above; an argument that names none is the same for every part. Nothing has to cross between parts.
All inputs are finite; a program needn't handle non-finite values.
Results may differ from a plain program's by a relative error of at most 0.03.
The roundings to bfloat16 on the way count: a program that leaves them out, or rounds other values in their place, can miss the bound.
Values may be sent and summed in bfloat16 or wider, within the bound.
A program may use at most 64 MiB of HBM per device.

v0:
```python
import jax
import jax.numpy as jnp
from jax import lax
from jax.sharding import PartitionSpec as P

HD = 64
WINDOW = 128
GRID_W = 64


EPS = 1e-06
THETA = 10000.0


def in_one_piece(arrays, axis, dim, along):
    both = jnp.concatenate(arrays, axis=along)
    filled, at, done = (lax.all_gather(both, axis, axis=dim, tiled=True), 0, [])
    for a in arrays:
        done.append(lax.slice_in_dim(filled, at, at + a.shape[along], axis=along))
        at += a.shape[along]
    return tuple(done)


def extended(block, sides, width):
    for axis, dim in sides:
        count = lax.axis_size(axis)
        forward = [(i, i + 1) for i in range(count - 1)]
        backward = [(target, source) for source, target in forward]
        low = lax.ppermute(
            lax.slice_in_dim(block, block.shape[dim] - width, None, axis=dim), axis, forward
        )
        high = lax.ppermute(lax.slice_in_dim(block, 0, width, axis=dim), axis, backward)
        block = jnp.concatenate([low, block, high], axis=dim)
    return block


def in_order(blocks, dim):
    lengths = list(blocks.shape[1:])
    lengths[dim] *= blocks.shape[0]
    return jnp.moveaxis(blocks, 0, dim).reshape(lengths)


def sent_to_all(x, axis):
    devices = lax.axis_size(axis)
    return lax.all_to_all(jnp.broadcast_to(x[None], (devices, *x.shape)), axis, 0, 0, tiled=True)


def gather_directly(x, axis, dim):
    return in_order(sent_to_all(x, axis), dim)


def rope_table(places, width):
    inverse = THETA ** (-jnp.arange(0, width, 2, dtype=jnp.float32) / width)
    angles = places.astype(jnp.float32)[:, None] * inverse[None, :]
    angles = jnp.concatenate([angles, angles], axis=-1)
    return (jnp.cos(angles), jnp.sin(angles))


def turn(values, tables):
    cosine, sine = tables
    middle = values.shape[-1] // 2
    rotated = jnp.concatenate([-values[..., middle:], values[..., :middle]], axis=-1)
    return values * cosine[:, None, :] + rotated * sine[:, None, :]


def head_norm(projected, gain):
    width = gain.shape[0]
    heads = projected.reshape(projected.shape[0], -1, width)
    return heads * lax.rsqrt(jnp.mean(heads * heads, axis=-1, keepdims=True) + EPS) * gain


def line_heads(projected, gain, places):
    normed = head_norm(projected, gain)
    turned = turn(normed, rope_table(places, gain.shape[0]))
    return turned.reshape(projected.shape).astype(jnp.bfloat16)


def grid_heads(projected, gain, places):
    normed = head_norm(projected, gain)
    middle = gain.shape[0] // 2
    by_row = turn(normed[..., :middle], rope_table(places // GRID_W, middle))
    by_col = turn(normed[..., middle:], rope_table(places % GRID_W, middle))
    joined = jnp.concatenate([by_row, by_col], axis=-1)
    return joined.reshape(projected.shape).astype(jnp.bfloat16)


def banded(query, keys_ext, values_ext, offset, total_len, sink_logit):
    length = query.shape[0]
    kv_heads = keys_ext.shape[1] // HD
    group_size = query.shape[1] // (HD * kv_heads)
    block_count = length // WINDOW
    query_blocks = query.reshape(block_count, WINDOW, kv_heads, group_size, HD)
    key_blocks = keys_ext.reshape(block_count + 2, WINDOW, kv_heads, HD)
    value_blocks = values_ext.reshape(block_count + 2, WINDOW, kv_heads, HD)
    key_near = jnp.concatenate([key_blocks[:-2], key_blocks[1:-1], key_blocks[2:]], axis=1)
    value_near = jnp.concatenate([value_blocks[:-2], value_blocks[1:-1], value_blocks[2:]], axis=1)
    scores = jnp.einsum(
        "nqhgd,nkhd->nhgqk", query_blocks, key_near, preferred_element_type=jnp.float32
    ) * HD ** (-0.5)
    query_pos = offset + jnp.arange(length, dtype=jnp.int32).reshape(block_count, WINDOW)
    key_pos = (
        offset
        - WINDOW
        + (
            jnp.arange(block_count, dtype=jnp.int32)[:, None] * WINDOW
            + jnp.arange(3 * WINDOW, dtype=jnp.int32)[None, :]
        )
    )
    valid = (
        (jnp.abs(query_pos[:, :, None] - key_pos[:, None, :]) <= WINDOW)
        & (key_pos >= 0)[:, None, :]
        & (key_pos < total_len)[:, None, :]
    )
    scores = jnp.where(valid[:, None, None], scores, -jnp.inf)
    floor = sink_logit.reshape(kv_heads, group_size)[None, :, :, None, None]
    top = jnp.maximum(jnp.max(scores, axis=-1, keepdims=True), floor)
    expon = jnp.exp(scores - top)
    weights = (expon / (jnp.sum(expon, axis=-1, keepdims=True) + jnp.exp(floor - top))).astype(
        jnp.bfloat16
    )
    result = jnp.einsum(
        "nhgqk,nkhd->nqhgd", weights, value_near, preferred_element_type=jnp.float32
    )
    return result.astype(jnp.bfloat16).reshape(length, -1)


def dense_whole(query, keys, values):
    length = query.shape[0]
    kv_heads = keys.shape[1] // HD
    group_size = query.shape[1] // (HD * kv_heads)
    block = 128
    query_blocks = query.reshape(length // block, block, kv_heads, group_size, HD)
    key_heads = keys.reshape(-1, kv_heads, HD)
    value_heads = values.reshape(-1, kv_heads, HD)

    def one_block(query_block):
        scores = jnp.einsum(
            "qhgd,khd->hgqk", query_block, key_heads, preferred_element_type=jnp.float32
        ) * HD ** (-0.5)
        top = jnp.max(scores, axis=-1, keepdims=True)
        expon = jnp.exp(scores - top)
        total = jnp.sum(expon, axis=-1)
        summed = jnp.einsum(
            "hgqk,khd->qhgd",
            expon.astype(jnp.bfloat16),
            value_heads,
            preferred_element_type=jnp.float32,
        )
        return (summed / jnp.transpose(total, (2, 0, 1))[..., None]).astype(jnp.bfloat16)

    result = lax.map(one_block, query_blocks)
    return result.reshape(length, -1)


def local(
    tokens_in,
    norm_gain,
    window_query,
    window_key,
    window_value,
    window_query_gain,
    window_key_gain,
    sink_logit,
    dense_query,
    dense_key,
    dense_value,
    dense_query_gain,
    dense_key_gain,
    window_out,
    dense_out,
):
    length = tokens_in.shape[0]
    inputs = tokens_in.astype(jnp.float32)
    normed = (
        inputs * lax.rsqrt(jnp.mean(inputs * inputs, axis=-1, keepdims=True) + EPS) * norm_gain
    ).astype(jnp.bfloat16)
    pieces = in_one_piece(
        (window_query, window_key, window_value, dense_query, dense_key, dense_value), "sp", 0, 1
    )
    projected = tuple(
        (jnp.dot(normed, weight, preferred_element_type=jnp.float32) for weight in pieces)
    )
    offset = lax.axis_index("sp") * length
    total_len = length * lax.axis_size("sp")
    places = offset + jnp.arange(length, dtype=jnp.int32)
    query_win = line_heads(projected[0], window_query_gain, places)
    key_win = line_heads(projected[1], window_key_gain, places)
    value_win = projected[2].astype(jnp.bfloat16)
    query_den = grid_heads(projected[3], dense_query_gain, places)
    key_den = grid_heads(projected[4], dense_key_gain, places)
    value_den = projected[5].astype(jnp.bfloat16)
    framed = extended(jnp.stack([key_win, value_win]), (("sp", 1),), WINDOW)
    att_win = banded(query_win, framed[0], framed[1], offset, total_len, sink_logit)
    dense_pair = jnp.stack([key_den, value_den])
    every = gather_directly(dense_pair, "sp", 1)
    att_den = dense_whole(query_den, every[0], every[1])
    columns = in_one_piece((window_out, dense_out), "sp", 1, 0)
    return lax.psum_scatter(
        (
            jnp.dot(att_win, columns[0], preferred_element_type=jnp.float32)
            + jnp.dot(att_den, columns[1], preferred_element_type=jnp.float32)
        ).astype(jnp.bfloat16),
        "tp",
        scatter_dimension=0,
        tiled=True,
    )


def solution(mesh):
    return jax.shard_map(
        local,
        mesh=mesh,
        in_specs=(
            P(("grp", "sp"), None),
            P(),
            P("sp", "tp"),
            P("sp", "tp"),
            P("sp", "tp"),
            P(),
            P(),
            P("tp"),
            P("sp", "tp"),
            P("sp", "tp"),
            P("sp", "tp"),
            P(),
            P(),
            P("tp", "sp"),
            P("tp", "sp"),
        ),
        out_specs=P(("grp", "sp", "tp"), None),
        check_vma=False,
    )
```

profile of v0, /device:TPU:33, one launch (start us, length us, event | category | flops | bytes accessed | tf_op | source)
XLA Modules:
  0.0 288.6 jit_solution(10850667919599419391)
XLA Ops:
  6.6 0.9 copy.58
  7.4 0.9 copy.59
  8.3 0.9 copy.60
  9.2 0.9 copy.61
  10.1 1.7 concatenate.132
  11.9 1.5 pad_maximum_fusion
  13.8 0.7 mul.383
  14.5 2.7 fusion.27
  17.3 0.7 fusion.81
  18.1 0.7 fusion.83
  18.9 1.2 fusion.29
  20.1 1.7 fusion.50
  21.8 72.1 %all-gather.3.cloned.1.call-done = bf16[4096,512]{1,0:T(8,128)(2,1)} async-done(((bf16[256,512]{1,0:T(8,128)(2,1)}), bf16[4096,512]{1,0:T(8,128)(2,1)}) %all-gather.3.cloned.1.call-update) | async-done | bytes 4194320 | tf_op jit(solution)/shard_map/all_gather | solution.py:17
  93.9 2.3 multiply_reduce_fusion.2
  96.5 2.7 fusion.33
  99.3 1.5 broadcast_in_dim.18
  100.8 6.7 %all-to-all-start = ((bf16[16,2,384,64]{2,3,1,0:T(8,128)(2,1)}), bf16[16,2,384,64]{2,3,1,0:T(8,128)(2,1)}, u32[]{:S(2)}, u32[]{:S(2)}) async-start(bf16[16,2,384,64]{2,3,1,0:T(8,128)(2,1)} %broadcast_in_dim.18), calls=%async_computation | async-start | bytes 3145728 | tf_op jit(solution)/shard_map/all_to_all | solution.py:45
  107.6 2.4 multiply_reduce_fusion.3
  110.3 1.5 convolution_convert_fusion.2
  111.9 0.6 pad_maximum_fusion.15
  112.5 3.7 %collective-permute-start = (bf16[2,128,64]{1,2,0:T(8,128)(2,1)}, bf16[2,128,64]{1,2,0:T(8,128)(2,1)}, u32[]{:S(2)}, u32[]{:S(2)}) collective-permute-start(bf16[2,128,64]{1,2,0:T(8,128)(2,1)} %get-tuple-element.82), channel_id=1, source_target_pairs={{0,8},{8,16},{16,24},{24,32},{32,40},{40,48},{48,56},{56,64},{64,7... | collective-permute-start | bytes 98312 | tf_op jit(solution)/shard_map/ppermute | solution.py:29
  116.2 1.5 collective-permute-start.1
  117.7 1.0 multiply_reduce_fusion.1
  118.8 1.1 multiply_reduce_fusion
  120.6 41.8 %collective-permute-done = bf16[2,128,64]{1,2,0:T(8,128)(2,1)} collective-permute-done((bf16[2,128,64]{1,2,0:T(8,128)(2,1)}, bf16[2,128,64]{1,2,0:T(8,128)(2,1)}, u32[]{:S(2)}, u32[]{:S(2)}) %collective-permute-start) | collective-permute-done | bytes 32800 | tf_op jit(solution)/shard_map/ppermute | solution.py:29
  162.4 22.4 %collective-permute-done.1 = bf16[2,128,64]{1,2,0:T(8,128)(2,1)} collective-permute-done((bf16[2,128,64]{1,2,0:T(8,128)(2,1)}, bf16[2,128,64]{1,2,0:T(8,128)(2,1)}, u32[]{:S(2)}, u32[]{:S(2)}) %collective-permute-start.1) | collective-permute-done | bytes 32800 | tf_op jit(solution)/shard_map/ppermute | solution.py:32
  184.8 0.8 pad_maximum_fusion.9
  185.8 0.4 fusion.104
  186.5 0.3 fusion.32
  187.0 28.4 %all-gather.5.cloned.1.call-done = bf16[256,4096]{1,0:T(8,128)(2,1)} async-done(((bf16[256,256]{1,0:T(8,128)(2,1)}), bf16[256,4096]{1,0:T(8,128)(2,1)}) %all-gather.5.cloned.1.call-update) | async-done | bytes 2097168 | tf_op jit(solution)/shard_map/all_gather | solution.py:17
  215.3 4.9 %fusion.40 = f32[384,4096]{1,0:T(8,128)} fusion(bf16[256,4096]{1,0:T(8,128)(2,1)} %all-gather.5.cloned.1.call-done, bf16[16,8,3,128]{3,2,1,0:T(4,128)(2,1)S(1)} %bitcast.185), kind=kOutput, calls=%fused_computation.40 | convolution fusion | flops 402653184 | bytes 7438336 | tf_op jit(solution)/shard_map/dot_general | solution.py:200
  220.3 1.5 fusion.103
  221.8 0.5 copy.72
  222.3 0.4 reshape_squeeze.9
  222.6 0.5 copy.71
  223.1 0.4 reshape_squeeze.8
  223.5 9.9 %while.10 = (s32[]{:T(128)}, bf16[3,128,1,2,64]{1,4,3,2,0:T(8,128)(2,1)S(1)}, bf16[3,128,1,2,64]{1,4,3,2,0:T(8,128)(2,1)S(1)}, bf16[6144,1,64]{0,2,1:T(8,128)(2,...) while((s32[]{:T(128)}, bf16[3,128,1,2,64]{1,4,3,2,0:T(8,128)(2,1)S(1)}, ...), condition=%wide.region_10.11_spmd, body=%wide.region_7.10_spmd.sunk | while | flops 412122624 | bytes 20517972 | solution.py:151
  223.5 1.1 fusion.118
  224.6 1.0 fusion.119
  225.6 1.2 fusion.120
  226.8 1.1 fusion.118
  227.9 1.0 fusion.119
  228.9 1.2 fusion.120
  230.1 1.1 fusion.118
  231.2 1.0 fusion.119
  232.2 1.2 fusion.120
  233.5 5.8 %add_convert_fusion = bf16[384,4096]{1,0:T(8,128)(2,1)} fusion(f32[384,4096]{1,0:T(8,128)} %fusion.40, bf16[256,4096]{1,0:T(8,128)(2,1)} %all-gather.5.cloned.1.call-done, bf16[16,8,3,128]{3,2,1,0:T(4,128)(2,1)S(1)} %bitcast.186), kind=kOutput, calls=%fused_computation.23 | convolution fusion | flops 405798912 | bytes 10584064 | tf_op jit(solution)/shard_map/dot_general | solution.py:201
  239.4 42.7 %reduce-scatter.2.cloned.1.call-done = bf16[48,4096]{1,0:T(8,128)(2,1)} async-done(((bf16[384,4096]{1,0:T(8,128)(2,1)}), bf16[48,4096]{1,0:T(8,128)(2,1)}) %reduce-scatter.2.cloned.1.call-update) | async-done | bytes 393232 | tf_op jit(solution)/shard_map/reduce_scatter | solution.py:198
  (88 shorter events, 2.6 us)
Async XLA Ops:
  6.5 12.3 %copy-start.8 = (f32[4096]{0:T(1024)S(1)}, f32[4096]{0:T(1024)}, u32[]{:S(2)}) copy-start(f32[4096]{0:T(1024)} %param.18) | copy-start | bytes 49156
  6.5 87.3 %all-gather.3.cloned.1.call-start = ((), (), s32[]{:S(2)}) async-start(), calls=%async_computation.2 | async-start | bytes 4456448 | tf_op jit(solution)/shard_map/all_gather | solution.py:17
  11.9 203.5 %all-gather.5.cloned.1.call-start = ((), (), s32[]{:S(2)}) async-start(), calls=%async_computation.3 | async-start | bytes 2228224 | tf_op jit(solution)/shard_map/all_gather | solution.py:17
  14.5 4.4 %copy-start = (bf16[384,4096]{1,0:T(8,128)(2,1)S(1)}, bf16[384,4096]{1,0:T(8,128)(2,1)}, u32[]{:S(2)}) copy-start(bf16[384,4096]{1,0:T(8,128)(2,1)} %param.17) | copy-start | bytes 9437188
  20.1 76.1 %copy-start.11 = (f32[64]{0:T(128)S(1)}, f32[64]{0:T(128)}, u32[]{:S(2)}) copy-start(f32[64]{0:T(128)} %param.29) | copy-start | bytes 772
  100.8 9.3 %copy-start.9 = (f32[64]{0:T(128)S(1)}, f32[64]{0:T(128)}, u32[]{:S(2)}) copy-start(f32[64]{0:T(128)} %param.23) | copy-start | bytes 772
  100.8 119.5 %all-to-all-start = ((bf16[16,2,384,64]{2,3,1,0:T(8,128)(2,1)}), bf16[16,2,384,64]{2,3,1,0:T(8,128)(2,1)}, u32[]{:S(2)}, u32[]{:S(2)}) async-start(bf16[16,2,384,64]{2,3,1,0:T(8,128)(2,1)} %broadcast_in_dim.18), calls=%async_computation | async-start | bytes 3145728 | tf_op jit(solution)/shard_map/all_to_all | solution.py:45
  107.5 174.6 %reduce-scatter.2.cloned.1.call-start = ((), (), s32[]{:S(2)}) async-start(), calls=%async_computation.4 | async-start | bytes 3538944 | tf_op jit(solution)/shard_map/reduce_scatter | solution.py:198
  107.6 2.8 copy-start.1
  112.5 49.9 %collective-permute-start = (bf16[2,128,64]{1,2,0:T(8,128)(2,1)}, bf16[2,128,64]{1,2,0:T(8,128)(2,1)}, u32[]{:S(2)}, u32[]{:S(2)}) collective-permute-start(bf16[2,128,64]{1,2,0:T(8,128)(2,1)} %get-tuple-element.82), channel_id=1, source_target_pairs={{0,8},{8,16},{16,24},{24,32},{32,40},{40,48},{48,56},{56,64},{64,7... | collective-permute-start | bytes 98312 | tf_op jit(solution)/shard_map/ppermute | solution.py:29
  116.2 68.6 %collective-permute-start.1 = (bf16[2,128,64]{1,2,0:T(8,128)(2,1)}, bf16[2,128,64]{1,2,0:T(8,128)(2,1)}, u32[]{:S(2)}, u32[]{:S(2)}) collective-permute-start(bf16[2,128,64]{1,2,0:T(8,128)(2,1)} %get-tuple-element.83), channel_id=1, source_target_pairs={{8,0},{16,8},{24,16},{32,24},{40,32},{48,40},{56,48},{64,56},{72,6... | collective-permute-start | bytes 98312 | tf_op jit(solution)/shard_map/ppermute | solution.py:32
  118.7 1.2 copy-start.12
  118.7 1.3 copy-start.13
  118.8 1.4 copy-start.2
  118.8 1.4 copy-start.3
  118.8 1.4 copy-start.4
  118.8 1.4 copy-start.5
  119.9 65.9 %copy-start.6 = (pred[3,128,384]{1,2,0:T(8,128)(4,1)S(1)}, pred[3,128,384]{1,2,0:T(8,128)(4,1)}, u32[]{:S(2)}) copy-start(pred[3,128,384]{1,2,0:T(8,128)(4,1)} %fusion.50) | copy-start | bytes 442372
  120.1 66.0 %copy-start.10 = (f32[2]{0:T(128)S(1)}, f32[2]{0:T(128)}, u32[]{:S(2)}) copy-start(f32[2]{0:T(128)} %param.24) | copy-start | bytes 28
  221.8 1.7 copy-start.7
Sparse Core Ops, SparseCore 0:
  12.0 81.8 all-gather.2
  95.6 119.6 all-gather.4
  239.5 42.4 reduce-scatter.1
where the time goes:
time: 290 us; the launch traced here: 289 us
  waiting for transfers between devices  208 us (72%)
  matrix products  29.3 us (10%)
  other arithmetic  14.8 us (5%)
  between operations  13.7 us (5%)
  starting transfers between devices  12 us (4%)
  local copies, waits for them, and re-layouts  11.1 us (4%)
    all_gather x2, waiting for transfers between devices, in_one_piece(): filled, at, done = (lax.all_gather(both, axis, axis=dim, tiled=True), 0, [])  101 us
    reduce_scatter x1, waiting for transfers between devices, local(): lax.psum_scatter((jnp.dot(att_win, columns[0], preferred_element_type=jnp...  42.7 us
    ppermute x1, waiting for transfers between devices, extended(): lax.ppermute(lax.slice_in_dim(block, block.shape[dim] - width, None, axis...  41.8 us
    ppermute x1, waiting for transfers between devices, extended(): lax.ppermute(lax.slice_in_dim(block, 0, width, axis=dim), axis, backward)  22.4 us
    dot_general x6, matrix products, local(): jnp.dot(normed, weight, preferred_element_type=jnp.float32)  11.1 us
    all_to_all x1, starting transfers between devices, sent_to_all(): lax.all_to_all(jnp.broadcast_to(x[None], (devices, *x.shape)), axis, 0, 0...  6.72 us
    dot_general x1, matrix products, local(): jnp.dot(att_den, columns[1], preferred_element_type=jnp.float32)  5.84 us
  transfers between devices with their start and end apart: 6, of which 5 were waited for; matrix products, arithmetic and copies ran while one was open for 11% of the time, Pallas kernels for 0%

commit v1 on v0

v1 whole, which is shorter than its diff:
```python
import functools

import jax
import jax.numpy as jnp
import numpy as np
from jax import lax
from jax.experimental import pallas as pl
from jax.experimental.pallas import tpu as pltpu
from jax.sharding import PartitionSpec as P

HD = 64
WINDOW = 128
GRID_W = 64
EPS = 1e-06
THETA = 10000.0
MESH = pl.DeviceIdType.MESH
F32 = jnp.float32
BF16 = jnp.bfloat16
LOW = -1e30
OUT_EARLY = 4


def nt(a, b):
    return lax.dot_general(a, b, (((1,), (1,)), ((), ())), preferred_element_type=F32)


def nn(a, b):
    return jnp.dot(a, b, preferred_element_type=F32)


def remote(src, dst, send, recv, device):
    return pltpu.make_async_remote_copy(
        src_ref=src, dst_ref=dst, send_sem=send, recv_sem=recv, device_id=device, device_id_type=MESH
    )


class Ring:
    def __init__(self, me, n, piece, send_sem, recv_sem):
        self.me, self.n, self.half = me, n, n // 2
        self.piece, self.send_sem, self.recv_sem = piece, send_sem, recv_sem
        self.to = ({"sp": lax.rem(me + 1, n)}, {"sp": lax.rem(me + n - 1, n)})

    def owner(self, way, step):
        shift = self.n - step if way == 0 else step
        return lax.rem(self.me + shift, self.n)

    def copy(self, way, step, p):
        ref = self.piece(self.owner(way, step), p)
        return remote(
            ref, ref, self.send_sem.at[way, step, p], self.recv_sem.at[way, step, p], self.to[way]
        )

    def send(self, way, step, p):
        self.copy(way, step, p).start()

    def wait(self, way, step, p):
        ref = self.piece(self.owner(way, step + 1), p)
        remote(
            ref, ref, self.send_sem.at[way, step, p], self.recv_sem.at[way, step, p], self.to[way]
        ).wait_recv()

    def begin(self):
        for p in range(2):
            for way in range(2):
                self.send(way, 0, p)

    def hop_piece(self, step, p):
        for way in range(2):
            self.wait(way, step - 1, p)

            @pl.when((step < self.half - 1) | (p == way))
            def _():
                self.send(way, step, p)

    def hop(self, step):
        for p in range(2):
            self.hop_piece(step, p)

    def last(self):
        for way in range(2):
            self.wait(way, self.half - 1, way)

    def drain(self):
        def body(step, carry):
            for way in range(2):
                for p in range(2):
                    self.copy(way, step, p).wait_send()
            return carry

        lax.fori_loop(0, self.half - 1, body, 0)
        for way in range(2):
            self.copy(way, self.half - 1, way).wait_send()


def kernel(
    n_sp, n_tp,
    tokens, gain, wq, wk, wv, wqg, wkg, sink, dq, dk, dv, dqg, dkg, wo, do, freq,
    out,
    x, wall, stage, acc, oall, kv, kvw, qd, qw, att, attw, m_s, l_s, a_s,
    table, dsend, drecv, mine, xs, r2, c1, rc, rd,
    lsem, in_s, in_r, kv_s, kv_r, out_s, out_r, halo_s, halo_r,
    d_s, d_r, x_s, x_r,
):
    me = lax.axis_index("sp")
    tp = lax.axis_index("tp")
    core = lax.rem(tp, 2)
    xc = lax.div(tp, 2)
    n_x = n_tp // 2
    length, width = x.shape
    depth = wall.shape[1]
    cols = oall.shape[2]
    half_rows = length // 2
    share = length // n_tp
    half = n_sp // 2
    right, left = {"sp": lax.rem(me + 1, n_sp)}, {"sp": lax.rem(me + n_sp - 1, n_sp)}
    partner = {"tp": xc * 2 + (1 - core)}
    x_up = {"tp": lax.rem(xc + 1, n_x) * 2 + core}
    x_down = {"tp": lax.rem(xc + n_x - 1, n_x) * 2 + core}

    barrier = pltpu.get_barrier_semaphore()
    for peer in (right, left, partner, x_up, x_down):
        pl.semaphore_signal(barrier, inc=1, device_id=peer, device_id_type=MESH)

    loads = [
        pltpu.make_async_copy(wk, stage.at[0], lsem.at[0]),
        pltpu.make_async_copy(wv, stage.at[1], lsem.at[1]),
        pltpu.make_async_copy(dk, stage.at[2], lsem.at[2]),
        pltpu.make_async_copy(dv, stage.at[3], lsem.at[3]),
        pltpu.make_async_copy(wq, wall.at[me, :, pl.ds(0, 128)], lsem.at[4]),
        pltpu.make_async_copy(dq, wall.at[me, :, pl.ds(256, 128)], lsem.at[5]),
        pltpu.make_async_copy(wo, oall.at[me, pl.ds(0, 128)], lsem.at[6]),
        pltpu.make_async_copy(do, oall.at[me, pl.ds(128, 128)], lsem.at[7]),
    ]
    for c in loads:
        c.start()
    quarter = length // 4
    token_loads = [
        pltpu.make_async_copy(
            tokens.at[pl.ds(i * quarter, quarter)], x.at[pl.ds(i * quarter, quarter)], lsem.at[8 + i]
        )
        for i in range(4)
    ]
    for c in token_loads:
        c.start()
    for c in loads[:4]:
        c.wait()
    for at, base in ((0, 128), (2, 384)):
        pair = jnp.concatenate([stage[at], stage[at + 1]], axis=0).astype(F32)
        wall[me, :, base : base + 128] = pair.T.astype(BF16)
    for c in loads[4:]:
        c.wait()
    pl.semaphore_wait(barrier, 5)

    rows2 = depth // 2
    in_ring = Ring(me, n_sp, lambda w, p: wall.at[w, pl.ds(p * rows2, rows2)], in_s, in_r)
    out_ring = Ring(me, n_sp, lambda w, p: oall.at[w, pl.ds(p * 128, 128)], out_s, out_r)
    kv_rows = length // 2
    kv_ring = Ring(me, n_sp, lambda w, p: kv.at[w, pl.ds(p * kv_rows, kv_rows)], kv_s, kv_r)
    in_ring.begin()

    for i in range(4):
        token_loads[i].wait()

        def norm_rows(r, carry):
            at = pl.multiple_of(i * quarter + r * 16, 16)
            total = jnp.zeros((16, 128), F32)
            for j in range(width // 128):
                piece = x[pl.ds(at, 16), j * 128 : j * 128 + 128].astype(F32)
                total = total + piece * piece
            scale = lax.rsqrt(jnp.sum(total, axis=-1, keepdims=True) * (1.0 / width) + EPS)
            for j in range(width // 128):
                piece = x[pl.ds(at, 16), j * 128 : j * 128 + 128].astype(F32)
                x[pl.ds(at, 16), j * 128 : j * 128 + 128] = (
                    piece * scale * gain[j : j + 1, :]
                ).astype(BF16)
            return carry

        lax.fori_loop(0, quarter // 16, norm_rows, 0)

    lane = lax.broadcasted_iota(jnp.int32, (1, 128), 1)
    low_lane = lane < HD

    def tables(r, carry):
        at = pl.multiple_of(r * 64, 64)
        place = me * length + at + lax.broadcasted_iota(jnp.int32, (64, 128), 0)
        angle = place.astype(F32) * freq[0:1, :]
        table[0, pl.ds(at, 64)] = jnp.cos(angle)
        table[1, pl.ds(at, 64)] = jnp.sin(angle)
        row = lax.div(place, GRID_W)
        spot = jnp.where(lax.rem(lane, HD) < HD // 2, row, place - row * GRID_W)
        angle = spot.astype(F32) * freq[1:2, :]
        table[2, pl.ds(at, 64)] = jnp.cos(angle)
        table[3, pl.ds(at, 64)] = jnp.sin(angle)
        return carry

    lax.fori_loop(0, length // 64, tables, 0)

    def project(w, first=False):
        at = pl.multiple_of(w * depth, depth)
        product = nn(x[:, pl.ds(at, depth)], wall[w])
        if first:
            acc[...] = product
        else:
            acc[...] += product

    project(me, first=True)

    def in_step(d, carry):
        in_ring.hop(d)
        project(in_ring.owner(0, d))
        project(in_ring.owner(1, d))
        return carry

    lax.fori_loop(1, half, in_step, 0)
    out_ring.begin()
    in_ring.last()
    project(in_ring.owner(0, half))

    def two(ref):
        return jnp.concatenate([ref[...], ref[...]], axis=1)

    def heads(values, g, which, reach, rows):
        squares = values * values
        low = jnp.sum(jnp.where(low_lane, squares, 0.0), axis=-1, keepdims=True)
        high = jnp.sum(jnp.where(low_lane, 0.0, squares), axis=-1, keepdims=True)
        mean = jnp.where(low_lane, low, high) * (1.0 / HD)
        normed = values * lax.rsqrt(mean + EPS) * g
        turned = jnp.where(
            lax.rem(lane, 2 * reach) < reach,
            -pltpu.roll(normed, 128 - reach, 1),
            pltpu.roll(normed, reach, 1),
        )
        return normed * table[which, rows] + turned * table[which + 1, rows]

    blocks = [slice(i * 128, i * 128 + 128) for i in range(length // 128)]
    g = two(dkg)
    for rows in blocks:
        values = acc[rows, 384:512]
        kv[me, rows] = jnp.where(low_lane, heads(values, g, 2, HD // 4, rows), values).astype(BF16)
    g = two(wkg)
    for i, rows in enumerate(blocks):
        values = acc[rows, 128:256]
        kvw[pl.ds(WINDOW + i * 128, 128)] = jnp.where(
            low_lane, heads(values, g, 0, HD // 2, rows), values
        ).astype(BF16)
    kv_ring.begin()
    halos = [
        remote(
            kvw.at[pl.ds(length, WINDOW)], kvw.at[pl.ds(0, WINDOW)], halo_s.at[0], halo_r.at[0], right
        ),
        remote(
            kvw.at[pl.ds(WINDOW, WINDOW)],
            kvw.at[pl.ds(WINDOW + length, WINDOW)],
            halo_s.at[1],
            halo_r.at[1],
            left,
        ),
    ]
    for c in halos:
        c.start()
    scale = HD ** (-0.5)
    for ref, base, gain_ref, which, reach in ((qd, 256, dqg, 2, HD // 4), (qw, 0, wqg, 0, HD // 2)):
        g = two(gain_ref)
        for rows in blocks:
            q = heads(acc[rows, base : base + 128], g, which, reach, rows).astype(BF16).astype(F32)
            q = q * scale
            ref[0, rows] = jnp.where(low_lane, q, 0.0).astype(BF16)
            ref[1, rows] = jnp.where(low_lane, pltpu.roll(q, HD, 1), 0.0).astype(BF16)

    m_s[...] = jnp.full(m_s.shape, LOW, F32)
    l_s[...] = jnp.zeros(l_s.shape, F32)
    a_s[...] = jnp.zeros(a_s.shape, F32)

    for c in halos:
        c.wait_recv()

    def window(i):
        at = pl.multiple_of(i * 128, 128)
        queries = jnp.concatenate([qw[0, pl.ds(at, 128)], qw[1, pl.ds(at, 128)]], axis=0)
        near = kvw[pl.ds(at, 3 * WINDOW)]
        scores = nt(queries, near)
        row = lax.broadcasted_iota(jnp.int32, scores.shape, 0)
        key = lax.broadcasted_iota(jnp.int32, scores.shape, 1)
        first = row < 128
        spot = jnp.where(first, row, row - 128)
        place = me * length + at - WINDOW + key
        valid = (
            (key >= spot)
            & (key <= spot + 2 * WINDOW)
            & (place >= 0)
            & (place < length * n_sp)
        )
        scores = jnp.where(valid, scores, LOW)
        floor = jnp.where(
            lax.broadcasted_iota(jnp.int32, (256, 1), 0) < 128, sink[0], sink[1]
        )
        top = jnp.maximum(jnp.max(scores, axis=-1, keepdims=True), floor)
        expon = jnp.exp(scores - top)
        total = jnp.sum(expon, axis=-1, keepdims=True) + jnp.exp(floor - top)
        weights = (expon / total).astype(BF16)
        result = nn(weights, near)
        attw[0, pl.ds(at, 128)] = jnp.where(
            low_lane, pltpu.roll(result[:128], HD, 1), result[128:]
        ).astype(BF16)

    def dense(owners, j):
        rows = pl.ds(j * 256, 256)
        queries = qd_rows(j)
        scores = [nt(queries, kv[w]) for w in owners]
        before = m_s[rows]
        top = before
        for s in scores:
            top = jnp.maximum(top, jnp.max(s, axis=-1, keepdims=True))
        shrink = jnp.exp(before - top)
        expons = [jnp.exp(s - top[:, :1]) for s in scores]
        total = l_s[rows] * shrink
        summed = a_s[rows] * shrink
        for e, w in zip(expons, owners):
            total = total + jnp.sum(e, axis=-1, keepdims=True)
            summed = summed + nn(e.astype(BF16), kv[w])
        m_s[rows] = top
        l_s[rows] = total
        a_s[rows] = summed

    def qd_rows(j):
        flat = [qd[0, 0:256], None, qd[1, 128:384]]
        if j == 1:
            return jnp.concatenate([qd[0, 256:384], qd[1, 0:128]], axis=0)
        return flat[j]

    def kv_step(d, carry):
        before = d - 1

        @pl.when(d < half)
        def _():
            kv_ring.hop_piece(d, 0)

        @pl.when(d >= 2)
        def _():
            dense((kv_ring.owner(0, before), kv_ring.owner(1, before)), 0)

        @pl.when(d < half)
        def _():
            kv_ring.hop_piece(d, 1)

        @pl.when(d >= 2)
        def _():
            dense((kv_ring.owner(0, before), kv_ring.owner(1, before)), 1)

        @pl.when((lax.rem(d, 2) == 0) & (d <= 2 * OUT_EARLY))
        def _():
            out_ring.hop(lax.div(d, 2))

        @pl.when(d >= 2)
        def _():
            dense((kv_ring.owner(0, before), kv_ring.owner(1, before)), 2)

        @pl.when(d <= length // 128)
        def _():
            window(d - 1)

        return carry

    lax.fori_loop(1, half + 1, kv_step, 0)
    kv_ring.last()
    for j in range(3):
        dense((me, kv_ring.owner(0, half)), j)

    for rows in blocks:
        first = a_s[rows] / l_s[rows]
        second_rows = slice(rows.start + length, rows.stop + length)
        second = a_s[second_rows] / l_s[second_rows]
        attw[1, rows] = jnp.where(low_lane, pltpu.roll(first, HD, 1), second).astype(BF16)
    for t in range(n_tp):
        at = (t % 2) * half_rows + (t // 2) * share
        for which in range(2):
            att[at : at + share, which * 128 : which * 128 + 128] = attw[
                which, t * share : t * share + share
            ]

    def owners_of(s):
        return (
            lax.rem(me + n_sp - lax.rem(s, half), n_sp),
            lax.rem(me + s, n_sp),
        )

    theirs_at = pl.multiple_of((1 - core) * half_rows, half_rows)
    mine_at = pl.multiple_of(core * half_rows, half_rows)
    up = lax.rem(xc + 1, n_x)
    down = lax.rem(xc + n_x - 1, n_x)
    far = lax.rem(xc + 2, n_x)
    ways = ((x_up, up, x_down, down), (x_down, down, x_up, up))

    def pair_copy(s):
        return remote(dsend.at[s], drecv.at[s], d_s.at[s], d_r.at[s], partner)

    def far_copy(s, b):
        return remote(xs.at[s, b, far], r2.at[s, b], x_s.at[0, s, b], x_r.at[0, s, b], ways[b][0])

    def chain_copy(s, b):
        return remote(c1.at[s, b], rc.at[s, b], x_s.at[1, s, b], x_r.at[1, s, b], ways[b][0])

    def near_copy(s, b):
        return remote(
            xs.at[s, b, ways[b][3]], rd.at[s, b], x_s.at[2, s, b], x_r.at[2, s, b], ways[b][2]
        )

    def stage1(s):
        owners = owners_of(s)
        for b in range(2):
            dsend[s - 1, b] = nn(att[pl.ds(theirs_at, half_rows)], oall[owners[b]]).astype(BF16)
        mine[s - 1, 0] = nn(att[pl.ds(mine_at, half_rows)], oall[owners[0]])
        pair_copy(s - 1).start()
        mine[s - 1, 1] = nn(att[pl.ds(mine_at, half_rows)], oall[owners[1]])

    def stage2(s):
        pair_copy(s - 1).wait_recv()
        for b in range(2):
            both = (mine[s - 1, b] + drecv[s - 1, b].astype(F32)).astype(BF16)
            for t in range(n_x):
                xs[s - 1, b, t] = both[t * share : t * share + share]
        for b in range(2):
            far_copy(s - 1, b).start()
        for b in range(2):
            near_copy(s - 1, b).start()

    def stage3(s):
        for b in range(2):
            far_copy(s - 1, b).wait_recv()
            c1[s - 1, b] = (xs[s - 1, b, ways[b][1]].astype(F32) + r2[s - 1, b].astype(F32)).astype(
                BF16
            )
        for b in range(2):
            chain_copy(s - 1, b).start()

    def stage4(s):
        owners = owners_of(s)
        for b in range(2):
            chain_copy(s - 1, b).wait_recv()
            near_copy(s - 1, b).wait_recv()
            total = (
                xs[s - 1, b, xc].astype(F32) + rc[s - 1, b].astype(F32) + rd[s - 1, b].astype(F32)
            )
            at = pl.multiple_of(owners[b] * cols, cols)
            out[:, pl.ds(at, cols)] = total.astype(BF16)

    def out_step(s, carry):
        @pl.when((s > OUT_EARLY) & (s < half))
        def _():
            out_ring.hop(s)

        @pl.when(s == half)
        def _():
            out_ring.last()

        @pl.when(s <= half)
        def _():
            stage1(s)

        @pl.when((s >= 2) & (s <= half + 1))
        def _():
            stage2(s - 1)

        @pl.when((s >= 3) & (s <= half + 2))
        def _():
            stage3(s - 2)

        @pl.when(s >= 4)
        def _():
            stage4(s - 3)

        return carry

    lax.fori_loop(1, half + 4, out_step, 0)

    for ring in (in_ring, kv_ring, out_ring):
        ring.drain()
    for c in halos:
        c.wait_send()

    def drain(s, carry):
        pair_copy(s).wait_send()
        for b in range(2):
            far_copy(s, b).wait_send()
            near_copy(s, b).wait_send()
            chain_copy(s, b).wait_send()
        return carry

    lax.fori_loop(0, half, drain, 0)


def frequencies():
    lane = np.arange(128)
    line = THETA ** (-2.0 * (lane % (HD // 2)) / HD)
    grid = THETA ** (-2.0 * (lane % (HD // 4)) / (HD // 2))
    return np.stack([line, grid]).astype(np.float32)


def solution(mesh):
    n_sp, n_tp = mesh.shape["sp"], mesh.shape["tp"]
    assert n_sp % 2 == 0 and n_tp == 8

    def local(tokens, gain, wq, wk, wv, wqg, wkg, sink, dq, dk, dv, dqg, dkg, wo, do):
        length, width = tokens.shape
        depth, cols = wq.shape[0], wo.shape[1]
        half, n_x, share = n_sp // 2, n_tp // 2, length // n_tp
        assert wq.shape[1] == dq.shape[1] == 2 * HD and wk.shape[1] == dk.shape[1] == HD
        assert length % 128 == 0 and share % 16 == 0 and width == depth * n_sp
        any_, vmem = pl.BlockSpec(memory_space=pl.ANY), pl.BlockSpec(memory_space=pltpu.VMEM)
        smem = pl.BlockSpec(memory_space=pltpu.SMEM)
        dma = pltpu.SemaphoreType.DMA
        return pl.pallas_call(
            functools.partial(kernel, n_sp, n_tp),
            out_shape=jax.ShapeDtypeStruct((share, cols * n_sp), BF16),
            in_specs=[any_, vmem, any_, any_, any_, vmem, vmem, smem, any_, any_, any_, vmem, vmem, any_, any_, vmem],
            out_specs=vmem,
            scratch_shapes=[
                pltpu.VMEM((length, width), BF16),
                pltpu.VMEM((n_sp, depth, 512), BF16),
                pltpu.VMEM((4, HD, depth), BF16),
                pltpu.VMEM((length, 512), F32),
                pltpu.VMEM((n_sp, 256, cols), BF16),
                pltpu.VMEM((n_sp, length, 128), BF16),
                pltpu.VMEM((length + 2 * WINDOW, 128), BF16),
                pltpu.VMEM((2, length, 128), BF16),
                pltpu.VMEM((2, length, 128), BF16),
                pltpu.VMEM((length, 256), BF16),
                pltpu.VMEM((2, length, 128), BF16),
                pltpu.VMEM((2 * length, 128), F32),
                pltpu.VMEM((2 * length, 128), F32),
                pltpu.VMEM((2 * length, 128), F32),
                pltpu.VMEM((4, length, 128), F32),
                pltpu.VMEM((half, 2, length // 2, cols), BF16),
                pltpu.VMEM((half, 2, length // 2, cols), BF16),
                pltpu.VMEM((half, 2, length // 2, cols), F32),
                pltpu.VMEM((half, 2, n_x, share, cols), BF16),
                pltpu.VMEM((half, 2, share, cols), BF16),
                pltpu.VMEM((half, 2, share, cols), BF16),
                pltpu.VMEM((half, 2, share, cols), BF16),
                pltpu.VMEM((half, 2, share, cols), BF16),
                dma((12,)),
                dma((2, half, 2)),
                dma((2, half, 2)),
                dma((2, half, 2)),
                dma((2, half, 2)),
                dma((2, half, 2)),
                dma((2, half, 2)),
                dma((2,)),
                dma((2,)),
                dma((half,)),
                dma((half,)),
                dma((3, half, 2)),
                dma((3, half, 2)),
            ],
            compiler_params=pltpu.CompilerParams(
                collective_id=0, has_side_effects=True, vmem_limit_bytes=60 * 1024 * 1024
            ),
        )(
            tokens, gain.reshape(-1, 128), wq, wk.T, wv.T, wqg[None], wkg[None], sink,
            dq, dk.T, dv.T, dqg[None], dkg[None], wo, do, jnp.asarray(frequencies()),
        )

    return jax.shard_map(
        local,
        mesh=mesh,
        in_specs=(
            P(("grp", "sp"), None),
            P(),
            P("sp", "tp"),
            P("sp", "tp"),
            P("sp", "tp"),
            P(),
            P(),
            P("tp"),
            P("sp", "tp"),
            P("sp", "tp"),
            P("sp", "tp"),
            P(),
            P(),
            P("tp", "sp"),
            P("tp", "sp"),
        ),
        out_specs=P(("grp", "sp", "tp"), None),
        check_vma=False,
    )
```

time: 290 us -> 145 us (0.50)
  waiting for transfers between devices: 208 us -> 0 us
  Pallas kernels: 0 us -> 143 us
  matrix products: 29.3 us -> 0 us
  other arithmetic: 14.8 us -> 0 us
  between operations: 13.7 us -> 0.01 us
  starting transfers between devices: 12 us -> 0 us
  local copies, waits for them, and re-layouts: 11.1 us -> 1.77 us
    pallas_call x0 -> x1, Pallas kernels: none -> 143 us  [local(): pl.pallas_call(functools.partial(kernel, n_sp, n_tp), out_shape=jax.Shape...]
    all_gather x2 -> x0, waiting for transfers between devices: 101 us -> none  [in_one_piece(): filled, at, done = (lax.all_gather(both, axis, axis=dim, tiled=True), 0, [])]
    ppermute x2 -> x0, waiting for transfers between devices: 64.2 us -> none  [the longest x1 41.8 us: extended(): lax.ppermute(lax.slice_in_dim(block, block.shape[dim] - width, None, axis...]
    reduce_scatter x1 -> x0, waiting for transfers between devices: 42.7 us -> none  [local(): lax.psum_scatter((jnp.dot(att_win, columns[0], preferred_element_type=jnp...]
    dot_general x16 -> x0, matrix products: 29.3 us -> none  [the longest x6 11.1 us: local(): jnp.dot(normed, weight, preferred_element_type=jnp.float32)]
    all_to_all x1 -> x0, starting transfers between devices: 6.72 us -> none  [sent_to_all(): lax.all_to_all(jnp.broadcast_to(x[None], (devices, *x.shape)), axis, 0, 0...]
    reduce_sum x5 -> x0, other arithmetic: 5.97 us -> none  [the longest x3 3.05 us: one_block(): total = jnp.sum(expon, axis=-1)]
    ppermute x2 -> x0, starting transfers between devices: 5.17 us -> none  [the longest x1 3.7 us: extended(): lax.ppermute(lax.slice_in_dim(block, block.shape[dim] - width, None, axis...]
  transfers between devices with their start and end apart: 6 -> 0, of which waited for: 5 -> 0; matrix products, arithmetic and copies ran while one was open for 11% -> 0% of each run, Pallas kernels for 0% -> 0%
where the time goes in v1:
time: 145 us; the launch traced here: 144 us
  Pallas kernels  143 us (99%)
  local copies, waits for them, and re-layouts  1.77 us (1%)
    pallas_call x1, Pallas kernels, local(): pl.pallas_call(functools.partial(kernel, n_sp, n_tp), out_shape=jax.Shape...  143 us

profile of v1, /device:TPU:33, one launch (start us, length us, event | category | flops | bytes accessed | tf_op | source)
XLA Modules:
  0.0 144.4 jit_solution(18347638014399990990)
XLA Ops:
  0.0 142.6 %shard_map.154 = bf16[48,4096]{1,0:T(8,128)(2,1)} custom-call(bf16[384,4096]{1,0:T(8,128)(2,1)} %tokens.1, f32[32,128]{1,0:T(8,128)} %bitcast.13, bf16[256,128]{1,0:T(8,128)(2,1)} %wq.1, bf16[64,256]{1,0:T(8,128)(2,1)} %bitcast.9, bf16[64,256]{1,0:T(8,128)(2,1)} %bitcast.10, f32[1,64]{1,0:T(1,128)} %bitcast.14, f32[1,64]{1,0:T(1,128)} %bitcast.15, f32[2]{0:T(128)} %sink.1, ...), custom_call_target="tpu_custom_call" | custom-call | tf_op jit(solution)/shard_map/pallas_call | solution.py:512
  142.6 1.8 %copy.18 = bf16[48,4096]{1,0:T(8,128)(2,1)} copy(bf16[48,4096]{1,0:T(8,128)(2,1)} %shard_map.154) | data formatting | bytes 786432

commit v2 on v1

--- a/solution.py
+++ b/solution.py
@@ -1,4 +1,5 @@
 import functools
+import math
 
 import jax
 import jax.numpy as jnp
@@ -17,7 +18,8 @@
 F32 = jnp.float32
 BF16 = jnp.bfloat16
 LOW = -1e30
-OUT_EARLY = 4
+OUT_EARLY = 8
+LAG = (1, 3, 5)
 
 
 def nt(a, b):
@@ -92,14 +94,63 @@
             self.copy(way, self.half - 1, way).wait_send()
 
 
+class PairRing(Ring):
+    def __init__(self, me, n, ref, give, side, other, send_sem, recv_sem, pair_send, pair_recv):
+        rows = ref.shape[1]
+        self.ref, self.give, self.other = ref, give, other
+        self.given_at = pl.multiple_of(side * (rows - give), 16)
+        self.taken_at = pl.multiple_of((1 - side) * (rows - give), 16)
+        self.pair_send, self.pair_recv = pair_send, pair_recv
+
+        def piece(w, p):
+            return ref.at[w, pl.ds(self.given_at, give) if p == 0 else pl.ds(give, rows - 2 * give)]
+
+        super().__init__(me, n, piece, send_sem, recv_sem)
+
+    def across(self, way, step, at):
+        ref = self.ref.at[self.owner(way, step), pl.ds(at, self.give)]
+        return remote(
+            ref, ref, self.pair_send.at[way, step - 1], self.pair_recv.at[way, step - 1], self.other
+        )
+
+    def hop_piece(self, step, p):
+        super().hop_piece(step, p)
+        if p == 0:
+            for way in range(2):
+                self.across(way, step, self.given_at).start()
+
+    def last(self):
+        self.wait(0, self.half - 1, 0)
+        self.across(0, self.half, self.given_at).start()
+        self.wait(1, self.half - 1, 1)
+
+    def take(self, step):
+        for way in range(2):
+            self.across(way, step, self.taken_at).wait_recv()
+
+    def take_last(self):
+        self.across(0, self.half, self.taken_at).wait_recv()
+
+    def drain(self):
+        super().drain()
+
+        def body(step, carry):
+            for way in range(2):
+                self.across(way, step, self.given_at).wait_send()
+            return carry
+
+        lax.fori_loop(1, self.half, body, 0)
+        self.across(0, self.half, self.given_at).wait_send()
+
+
 def kernel(
     n_sp, n_tp,
     tokens, gain, wq, wk, wv, wqg, wkg, sink, dq, dk, dv, dqg, dkg, wo, do, freq,
     out,
-    x, wall, stage, acc, oall, kv, kvw, qd, qw, att, attw, m_s, l_s, a_s,
+    x, wall, stage, acc, oall, kp, vt, kvw, qd, qw, att, attw, m_s, a_s,
     table, dsend, drecv, mine, xs, r2, c1, rc, rd,
     lsem, in_s, in_r, kv_s, kv_r, out_s, out_r, halo_s, halo_r,
-    d_s, d_r, x_s, x_r,
+    d_s, d_r, x_s, x_r, in_ys, in_yr, out_ys, out_yr, held, o_s,
 ):
     me = lax.axis_index("sp")
     tp = lax.axis_index("tp")
@@ -117,8 +168,12 @@
     x_up = {"tp": lax.rem(xc + 1, n_x) * 2 + core}
     x_down = {"tp": lax.rem(xc + n_x - 1, n_x) * 2 + core}
 
+    grp = lax.axis_index("grp")
+    side = lax.rem(grp, 2)
+    other = {"grp": grp + 1 - 2 * side}
+
     barrier = pltpu.get_barrier_semaphore()
-    for peer in (right, left, partner, x_up, x_down):
+    for peer in (right, left, partner, x_up, x_down, other):
         pl.semaphore_signal(barrier, inc=1, device_id=peer, device_id_type=MESH)
 
     loads = [
@@ -149,16 +204,14 @@
         wall[me, :, base : base + 128] = pair.T.astype(BF16)
     for c in loads[4:]:
         c.wait()
-    pl.semaphore_wait(barrier, 5)
-
-    rows2 = depth // 2
-    in_ring = Ring(me, n_sp, lambda w, p: wall.at[w, pl.ds(p * rows2, rows2)], in_s, in_r)
-    out_ring = Ring(me, n_sp, lambda w, p: oall.at[w, pl.ds(p * 128, 128)], out_s, out_r)
-    kv_rows = length // 2
-    kv_ring = Ring(me, n_sp, lambda w, p: kv.at[w, pl.ds(p * kv_rows, kv_rows)], kv_s, kv_r)
+    pl.semaphore_wait(barrier, 6)
+
+    in_ring = PairRing(me, n_sp, wall, depth * 5 // 16, side, other, in_s, in_r, in_ys, in_yr)
+    out_ring = PairRing(me, n_sp, oall, 80, side, other, out_s, out_r, out_ys, out_yr)
+    kv_ring = Ring(me, n_sp, lambda w, p: (kp, vt)[p].at[w], kv_s, kv_r)
     in_ring.begin()
 
-    for i in range(4):
+    def norm(i):
         token_loads[i].wait()
 
         def norm_rows(r, carry):
@@ -193,8 +246,6 @@
         table[3, pl.ds(at, 64)] = jnp.sin(angle)
         return carry
 
-    lax.fori_loop(0, length // 64, tables, 0)
-
     def project(w, first=False):
         at = pl.multiple_of(w * depth, depth)
         product = nn(x[:, pl.ds(at, depth)], wall[w])
@@ -203,17 +254,43 @@
         else:
             acc[...] += product
 
-    project(me, first=True)
-
-    def in_step(d, carry):
-        in_ring.hop(d)
+    def projects(d, carry):
+        in_ring.take(d)
         project(in_ring.owner(0, d))
         project(in_ring.owner(1, d))
         return carry
 
+    def in_step(d, carry):
+        in_ring.hop(d)
+
+        @pl.when(d == 1)
+        def _():
+            norm(0)
+            norm(1)
+
+        @pl.when(d == 2)
+        def _():
+            norm(2)
+            norm(3)
+
+        @pl.when(d == 3)
+        def _():
+            lax.fori_loop(0, length // 64, tables, 0)
+            project(me, first=True)
+
+        @pl.when(d >= 4)
+        def _():
+            lax.fori_loop(
+                jnp.where(d < 6, 2 * d - 7, d - 1), jnp.where(d < 6, 2 * d - 5, d), projects, 0
+            )
+
+        return carry
+
     lax.fori_loop(1, half, in_step, 0)
     out_ring.begin()
     in_ring.last()
+    projects(half - 1, 0)
+    in_ring.take_last()
     project(in_ring.owner(0, half))
 
     def two(ref):
@@ -234,9 +311,13 @@
 
     blocks = [slice(i * 128, i * 128 + 128) for i in range(length // 128)]
     g = two(dkg)
+    keys = [
+        heads(acc[rows, 384:512], g, 2, HD // 4, rows)
+        for rows in (slice(0, half_rows), slice(half_rows, length))
+    ]
+    kp[me] = jnp.where(low_lane, keys[0], pltpu.roll(keys[1], HD, 1)).astype(BF16)
     for rows in blocks:
-        values = acc[rows, 384:512]
-        kv[me, rows] = jnp.where(low_lane, heads(values, g, 2, HD // 4, rows), values).astype(BF16)
+        vt[me, :, rows] = acc[rows, 384:512].T[HD:].astype(BF16)
     g = two(wkg)
     for i, rows in enumerate(blocks):
         values = acc[rows, 128:256]
@@ -259,20 +340,23 @@
     for c in halos:
         c.start()
     scale = HD ** (-0.5)
-    for ref, base, gain_ref, which, reach in ((qd, 256, dqg, 2, HD // 4), (qw, 0, wqg, 0, HD // 2)):
-        g = two(gain_ref)
-        for rows in blocks:
-            q = heads(acc[rows, base : base + 128], g, which, reach, rows).astype(BF16).astype(F32)
-            q = q * scale
-            ref[0, rows] = jnp.where(low_lane, q, 0.0).astype(BF16)
-            ref[1, rows] = jnp.where(low_lane, pltpu.roll(q, HD, 1), 0.0).astype(BF16)
+    g = two(dqg)
+    for rows in blocks:
+        q = heads(acc[rows, 256:384], g, 2, HD // 4, rows) * (scale * math.log2(math.e))
+        q = q.T.astype(BF16)
+        for h in range(2):
+            for p in range(2):
+                cols_h = slice(h * length + rows.start, h * length + rows.stop)
+                qd[p, p * HD : p * HD + HD, cols_h] = q[h * HD : h * HD + HD]
+                qd[p, (1 - p) * HD : (1 - p) * HD + HD, cols_h] = jnp.zeros((HD, 128), BF16)
+    g = two(wqg)
+    for rows in blocks:
+        q = heads(acc[rows, 0:128], g, 0, HD // 2, rows).astype(BF16).astype(F32) * scale
+        qw[0, rows] = jnp.where(low_lane, q, 0.0).astype(BF16)
+        qw[1, rows] = jnp.where(low_lane, pltpu.roll(q, HD, 1), 0.0).astype(BF16)
 
     m_s[...] = jnp.full(m_s.shape, LOW, F32)
-    l_s[...] = jnp.zeros(l_s.shape, F32)
     a_s[...] = jnp.zeros(a_s.shape, F32)
-
-    for c in halos:
-        c.wait_recv()
 
     def window(i):
         at = pl.multiple_of(i * 128, 128)
@@ -303,74 +387,62 @@
             low_lane, pltpu.roll(result[:128], HD, 1), result[128:]
         ).astype(BF16)
 
-    def dense(owners, j):
-        rows = pl.ds(j * 256, 256)
-        queries = qd_rows(j)
-        scores = [nt(queries, kv[w]) for w in owners]
-        before = m_s[rows]
-        top = before
-        for s in scores:
-            top = jnp.maximum(top, jnp.max(s, axis=-1, keepdims=True))
-        shrink = jnp.exp(before - top)
-        expons = [jnp.exp(s - top[:, :1]) for s in scores]
-        total = l_s[rows] * shrink
-        summed = a_s[rows] * shrink
-        for e, w in zip(expons, owners):
-            total = total + jnp.sum(e, axis=-1, keepdims=True)
-            summed = summed + nn(e.astype(BF16), kv[w])
-        m_s[rows] = top
-        l_s[rows] = total
-        a_s[rows] = summed
-
-    def qd_rows(j):
-        flat = [qd[0, 0:256], None, qd[1, 128:384]]
-        if j == 1:
-            return jnp.concatenate([qd[0, 256:384], qd[1, 0:128]], axis=0)
-        return flat[j]
+    ones = jnp.ones((8, 2 * length), BF16)
+
+    def dense(owners):
+        keys = jnp.concatenate([kp[w] for w in owners], axis=0)
+        values = jnp.concatenate(
+            [jnp.concatenate([vt[w] for w in owners], axis=1), ones], axis=0
+        )
+        low, high = nn(keys, qd[0]), nn(keys, qd[1])
+        before = m_s[...]
+        top = jnp.maximum(before, jnp.max(jnp.maximum(low, high), axis=0, keepdims=True))
+        shrink = jnp.exp2(before - top)
+        low = jnp.exp2(low - top[:1]).astype(BF16)
+        high = jnp.exp2(high - top[:1]).astype(BF16)
+        expons = jnp.concatenate(
+            [low[:half_rows], high[:half_rows], low[half_rows:], high[half_rows:]], axis=0
+        )
+        a_s[...] = a_s[...] * shrink[:1] + nn(values, expons)
+        m_s[...] = top
 
     def kv_step(d, carry):
-        before = d - 1
-
         @pl.when(d < half)
         def _():
-            kv_ring.hop_piece(d, 0)
+            kv_ring.hop(d)
+
+        @pl.when((d <= OUT_EARLY) & (d < half))
+        def _():
+            out_ring.hop(d)
+
+        @pl.when((d == OUT_EARLY) & (d == half))
+        def _():
+            out_ring.last()
 
         @pl.when(d >= 2)
         def _():
-            dense((kv_ring.owner(0, before), kv_ring.owner(1, before)), 0)
-
-        @pl.when(d < half)
-        def _():
-            kv_ring.hop_piece(d, 1)
-
-        @pl.when(d >= 2)
-        def _():
-            dense((kv_ring.owner(0, before), kv_ring.owner(1, before)), 1)
-
-        @pl.when((lax.rem(d, 2) == 0) & (d <= 2 * OUT_EARLY))
-        def _():
-            out_ring.hop(lax.div(d, 2))
-
-        @pl.when(d >= 2)
-        def _():
-            dense((kv_ring.owner(0, before), kv_ring.owner(1, before)), 2)
-
-        @pl.when(d <= length // 128)
-        def _():
-            window(d - 1)
+            dense((kv_ring.owner(0, d - 1), kv_ring.owner(1, d - 1)))
+
+        @pl.when(d == 3)
+        def _():
+            for c in halos:
+                c.wait_recv()
+
+        @pl.when((d >= 3) & (d < 3 + length // 128))
+        def _():
+            window(d - 3)
 
         return carry
 
     lax.fori_loop(1, half + 1, kv_step, 0)
     kv_ring.last()
-    for j in range(3):
-        dense((me, kv_ring.owner(0, half)), j)
-
+    dense((me, kv_ring.owner(0, half)))
+    both = jnp.concatenate(
+        [a_s[:HD, h * length : h * length + length] / a_s[HD : HD + 1, h * length : h * length + length] for h in range(2)],
+        axis=0,
+    )
     for rows in blocks:
-        first = a_s[rows] / l_s[rows]
-        second_rows = slice(rows.start + length, rows.stop + length)
-        second = a_s[second_rows] / l_s[second_rows]
-        attw[1, rows] = jnp.where(low_lane, pltpu.roll(first, HD, 1), second).astype(BF16)
+        attw[1, rows] = both[:, rows].T.astype(BF16)
     for t in range(n_tp):
         at = (t % 2) * half_rows + (t // 2) * share
         for which in range(2):
@@ -405,6 +477,10 @@
             xs.at[s, b, ways[b][3]], rd.at[s, b], x_s.at[2, s, b], x_r.at[2, s, b], ways[b][2]
         )
 
+    def put(s, b):
+        at = pl.multiple_of(owners_of(s)[b] * cols, cols)
+        return pltpu.make_async_copy(held.at[s - 1, b], out.at[:, pl.ds(at, cols)], o_s.at[s - 1, b])
+
     def stage1(s):
         owners = owners_of(s)
         for b in range(2):
@@ -434,49 +510,63 @@
             chain_copy(s - 1, b).start()
 
     def stage4(s):
-        owners = owners_of(s)
         for b in range(2):
             chain_copy(s - 1, b).wait_recv()
             near_copy(s - 1, b).wait_recv()
             total = (
                 xs[s - 1, b, xc].astype(F32) + rc[s - 1, b].astype(F32) + rd[s - 1, b].astype(F32)
             )
-            at = pl.multiple_of(owners[b] * cols, cols)
-            out[:, pl.ds(at, cols)] = total.astype(BF16)
+            held[s - 1, b] = total.astype(BF16)
+        for b in range(2):
+            put(s, b).start()
 
     def out_step(s, carry):
-        @pl.when((s > OUT_EARLY) & (s < half))
-        def _():
-            out_ring.hop(s)
+        ahead = s + OUT_EARLY
+
+        @pl.when(ahead < half)
+        def _():
+            out_ring.hop(ahead)
+
+        @pl.when(ahead == half)
+        def _():
+            out_ring.last()
+
+        @pl.when(s < half)
+        def _():
+            out_ring.take(s)
 
         @pl.when(s == half)
         def _():
-            out_ring.last()
+            out_ring.take_last()
 
         @pl.when(s <= half)
         def _():
             stage1(s)
 
-        @pl.when((s >= 2) & (s <= half + 1))
-        def _():
-            stage2(s - 1)
-
-        @pl.when((s >= 3) & (s <= half + 2))
-        def _():
-            stage3(s - 2)
-
-        @pl.when(s >= 4)
-        def _():
-            stage4(s - 3)
+        @pl.when((s >= 1 + LAG[0]) & (s <= half + LAG[0]))
+        def _():
+            stage2(s - LAG[0])
+
+        @pl.when((s >= 1 + LAG[1]) & (s <= half + LAG[1]))
+        def _():
+            stage3(s - LAG[1])
+
+        @pl.when(s >= 1 + LAG[2])
+        def _():
+            stage4(s - LAG[2])
+
+        @pl.when(s == 3)
+        def _():
+            in_ring.drain()
+            kv_ring.drain()
+            for c in halos:
+                c.wait_send()
 
         return carry
 
-    lax.fori_loop(1, half + 4, out_step, 0)
-
-    for ring in (in_ring, kv_ring, out_ring):
-        ring.drain()
-    for c in halos:
-        c.wait_send()
+    lax.fori_loop(1, half + LAG[2] + 1, out_step, 0)
+
+    out_ring.drain()
 
     def drain(s, carry):
         pair_copy(s).wait_send()
@@ -484,6 +574,7 @@
             far_copy(s, b).wait_send()
             near_copy(s, b).wait_send()
             chain_copy(s, b).wait_send()
+            put(s + 1, b).wait()
         return carry
 
     lax.fori_loop(0, half, drain, 0)
@@ -498,7 +589,7 @@
 
 def solution(mesh):
     n_sp, n_tp = mesh.shape["sp"], mesh.shape["tp"]
-    assert n_sp % 2 == 0 and n_tp == 8
+    assert n_sp % 2 == 0 and n_tp == 8 and mesh.shape["grp"] % 2 == 0
 
     def local(tokens, gain, wq, wk, wv, wqg, wkg, sink, dq, dk, dv, dqg, dkg, wo, do):
         length, width = tokens.shape
@@ -513,22 +604,22 @@
             functools.partial(kernel, n_sp, n_tp),
             out_shape=jax.ShapeDtypeStruct((share, cols * n_sp), BF16),
             in_specs=[any_, vmem, any_, any_, any_, vmem, vmem, smem, any_, any_, any_, vmem, vmem, any_, any_, vmem],
-            out_specs=vmem,
+            out_specs=any_,
             scratch_shapes=[
                 pltpu.VMEM((length, width), BF16),
                 pltpu.VMEM((n_sp, depth, 512), BF16),
                 pltpu.VMEM((4, HD, depth), BF16),
                 pltpu.VMEM((length, 512), F32),
                 pltpu.VMEM((n_sp, 256, cols), BF16),
-                pltpu.VMEM((n_sp, length, 128), BF16),
+                pltpu.VMEM((n_sp, length // 2, 128), BF16),
+                pltpu.VMEM((n_sp, HD, length), BF16),
                 pltpu.VMEM((length + 2 * WINDOW, 128), BF16),
-                pltpu.VMEM((2, length, 128), BF16),
+                pltpu.VMEM((2, 128, 2 * length), BF16),
                 pltpu.VMEM((2, length, 128), BF16),
                 pltpu.VMEM((length, 256), BF16),
                 pltpu.VMEM((2, length, 128), BF16),
-                pltpu.VMEM((2 * length, 128), F32),
-                pltpu.VMEM((2 * length, 128), F32),
-                pltpu.VMEM((2 * length, 128), F32),
+                pltpu.VMEM((8, 2 * length), F32),
+                pltpu.VMEM((HD + 8, 2 * length), F32),
                 pltpu.VMEM((4, length, 128), F32),
                 pltpu.VMEM((half, 2, length // 2, cols), BF16),
                 pltpu.VMEM((half, 2, length // 2, cols), BF16),
@@ -551,6 +642,12 @@
                 dma((half,)),
                 dma((3, half, 2)),
                 dma((3, half, 2)),
+                dma((2, half)),
+                dma((2, half)),
+                dma((2, half)),
+                dma((2, half)),
+                pltpu.VMEM((half, 2, share, cols), BF16),
+                dma((half, 2)),
             ],
             compiler_params=pltpu.CompilerParams(
                 collective_id=0, has_side_effects=True, vmem_limit_bytes=60 * 1024 * 1024

time: 145 us -> 124 us (0.86)
  Pallas kernels: 143 us -> 122 us
    pallas_call x1, Pallas kernels: 143 us -> 122 us  [local(): pl.pallas_call(functools.partial(kernel, n_sp, n_tp), out_shape=jax.Shape...]
where the time goes in v2:
time: 124 us
  Pallas kernels  122 us (98%)
  local copies, waits for them, and re-layouts  1.77 us (1%)
    pallas_call x1, Pallas kernels, local(): pl.pallas_call(functools.partial(kernel, n_sp, n_tp), out_shape=jax.Shape...  122 us

profile of v2, /device:TPU:33, one launch (start us, length us, event | category | flops | bytes accessed | tf_op | source)
XLA Modules:
  0.0 123.8 jit_solution(3166929083773082060)
XLA Ops:
  0.0 122.1 %shard_map.154 = bf16[48,4096]{1,0:T(8,128)(2,1)} custom-call(bf16[384,4096]{1,0:T(8,128)(2,1)} %tokens.1, f32[32,128]{1,0:T(8,128)} %bitcast.13, bf16[256,128]{1,0:T(8,128)(2,1)} %wq.1, bf16[64,256]{1,0:T(8,128)(2,1)} %bitcast.9, bf16[64,256]{1,0:T(8,128)(2,1)} %bitcast.10, f32[1,64]{1,0:T(1,128)} %bitcast.14, f32[1,64]{1,0:T(1,128)} %bitcast.15, f32[2]{0:T(128)} %sink.1, ...), custom_call_target="tpu_custom_call" | custom-call | tf_op jit(solution)/shard_map/pallas_call | solution.py:603
  122.1 1.8 %copy.18 = bf16[48,4096]{1,0:T(8,128)(2,1)} copy(bf16[48,4096]{1,0:T(8,128)(2,1)} %shard_map.154) | data formatting | bytes 786432

commit v3 on v2

--- a/solution.py
+++ b/solution.py
@@ -18,8 +18,7 @@
 F32 = jnp.float32
 BF16 = jnp.bfloat16
 LOW = -1e30
-OUT_EARLY = 8
-LAG = (1, 3, 5)
+LAG = (1, 5, 2, 13)
 
 
 def nt(a, b):
@@ -37,8 +36,10 @@
 
 
 class Ring:
-    def __init__(self, me, n, piece, send_sem, recv_sem):
+    def __init__(self, me, n, count, piece, send_sem, recv_sem, place=0):
+        self.place = place
         self.me, self.n, self.half = me, n, n // 2
+        self.count = count
         self.piece, self.send_sem, self.recv_sem = piece, send_sem, recv_sem
         self.to = ({"sp": lax.rem(me + 1, n)}, {"sp": lax.rem(me + n - 1, n)})
 
@@ -46,83 +47,111 @@
         shift = self.n - step if way == 0 else step
         return lax.rem(self.me + shift, self.n)
 
-    def copy(self, way, step, p):
-        ref = self.piece(self.owner(way, step), p)
+    def copy(self, way, step, p, distance):
+        ref = self.piece(self.owner(way, distance), p)
         return remote(
-            ref, ref, self.send_sem.at[way, step, p], self.recv_sem.at[way, step, p], self.to[way]
+            ref, ref, self.send_sem.at[way, lax.rem(step, 2), p], self.recv_sem.at[way, step, self.place + p], self.to[way]
         )
 
     def send(self, way, step, p):
-        self.copy(way, step, p).start()
+        @pl.when(step >= 2)
+        def _():
+            self.copy(way, step - 2, p, step - 2).wait_send()
+
+        self.copy(way, step, p, step).start()
 
     def wait(self, way, step, p):
-        ref = self.piece(self.owner(way, step + 1), p)
-        remote(
-            ref, ref, self.send_sem.at[way, step, p], self.recv_sem.at[way, step, p], self.to[way]
-        ).wait_recv()
+        self.copy(way, step, p, step + 1).wait_recv()
+
+    def way_of(self, p):
+        return 2 * p // self.count
 
     def begin(self):
-        for p in range(2):
+        for p in range(self.count):
             for way in range(2):
-                self.send(way, 0, p)
+                self.copy(way, 0, p, 0).start()
 
     def hop_piece(self, step, p):
         for way in range(2):
             self.wait(way, step - 1, p)
 
-            @pl.when((step < self.half - 1) | (p == way))
+            @pl.when((step < self.half - 1) | (self.way_of(p) == way))
             def _():
                 self.send(way, step, p)
 
-    def hop(self, step):
-        for p in range(2):
-            self.hop_piece(step, p)
+    def wait_last(self, way):
+        for p in range(self.count):
+            if self.way_of(p) == way:
+                self.wait(way, self.half - 1, p)
 
     def last(self):
         for way in range(2):
-            self.wait(way, self.half - 1, way)
+            self.wait_last(way)
 
     def drain(self):
-        def body(step, carry):
-            for way in range(2):
-                for p in range(2):
-                    self.copy(way, step, p).wait_send()
-            return carry
-
-        lax.fori_loop(0, self.half - 1, body, 0)
         for way in range(2):
-            self.copy(way, self.half - 1, way).wait_send()
+            for p in range(self.count):
+                final = self.half - 1 if self.way_of(p) == way else self.half - 2
+                for step in (final - 1, final):
+                    self.copy(way, step, p, step).wait_send()
 
 
 class PairRing(Ring):
     def __init__(self, me, n, ref, give, side, other, send_sem, recv_sem, pair_send, pair_recv):
         rows = ref.shape[1]
+        common = rows - 2 * give
         self.ref, self.give, self.other = ref, give, other
         self.given_at = pl.multiple_of(side * (rows - give), 16)
         self.taken_at = pl.multiple_of((1 - side) * (rows - give), 16)
         self.pair_send, self.pair_recv = pair_send, pair_recv
+        if common:
+            first = give // 32 * 16
+            cuts = [(0, first), (first, give - first)]
+            later = [(give, common // 2), (give + common // 2, common - common // 2)]
+        else:
+            cuts, later = [(0, give // 2), (give // 2, give // 2)], []
+        self.cross_after = 1
+        self.early_cross = bool(later)
 
         def piece(w, p):
-            return ref.at[w, pl.ds(self.given_at, give) if p == 0 else pl.ds(give, rows - 2 * give)]
-
-        super().__init__(me, n, piece, send_sem, recv_sem)
+            if p < 2:
+                at = pl.multiple_of(self.given_at + cuts[p][0], 16)
+                return ref.at[w, pl.ds(at, cuts[p][1])]
+            return ref.at[w, pl.ds(*later[p - 2])]
+
+        super().__init__(me, n, 2 + len(later), piece, send_sem, recv_sem, 0 if later else 2)
 
     def across(self, way, step, at):
         ref = self.ref.at[self.owner(way, step), pl.ds(at, self.give)]
         return remote(
-            ref, ref, self.pair_send.at[way, step - 1], self.pair_recv.at[way, step - 1], self.other
+            ref, ref, self.pair_send.at[way, lax.rem(step, 2)], self.pair_recv.at[way, step - 1], self.other
         )
 
     def hop_piece(self, step, p):
         super().hop_piece(step, p)
-        if p == 0:
+        if p == self.cross_after:
             for way in range(2):
+
+                @pl.when(step >= 3)
+                def _():
+                    self.across(way, step - 2, self.given_at).wait_send()
+
                 self.across(way, step, self.given_at).start()
 
+    def last_first(self):
+        self.wait_last(0)
+        if not self.early_cross:
+            self.wait_last(1)
+        self.across(0, self.half - 2, self.given_at).wait_send()
+        self.across(0, self.half, self.given_at).start()
+
+    def last_second(self):
+        if self.early_cross:
+            self.wait_last(1)
+
     def last(self):
-        self.wait(0, self.half - 1, 0)
-        self.across(0, self.half, self.given_at).start()
-        self.wait(1, self.half - 1, 1)
+        self.last_first()
+        self.last_second()
 
     def take(self, step):
         for way in range(2):
@@ -133,24 +162,21 @@
 
     def drain(self):
         super().drain()
-
-        def body(step, carry):
-            for way in range(2):
-                self.across(way, step, self.given_at).wait_send()
-            return carry
-
-        lax.fori_loop(1, self.half, body, 0)
         self.across(0, self.half, self.given_at).wait_send()
+        for way in range(2):
+            self.across(way, self.half - 1, self.given_at).wait_send()
+        self.across(1, self.half - 2, self.given_at).wait_send()
 
 
 def kernel(
     n_sp, n_tp,
-    tokens, gain, wq, wk, wv, wqg, wkg, sink, dq, dk, dv, dqg, dkg, wo, do, freq,
+    tokens, gain_h, wq, wk, wv, wqg_h, wkg_h, sink, dq, dk, dv, dqg_h, dkg_h, wo, do, freq_h,
     out,
     x, wall, stage, acc, oall, kp, vt, kvw, qd, qw, att, attw, m_s, a_s,
     table, dsend, drecv, mine, xs, r2, c1, rc, rd,
-    lsem, in_s, in_r, kv_s, kv_r, out_s, out_r, halo_s, halo_r,
+    lsem, in_s, in_r, out_s, halo_s, halo_r,
     d_s, d_r, x_s, x_r, in_ys, in_yr, out_ys, out_yr, held, o_s,
+    gain, gains, freq, kv_snd,
 ):
     me = lax.axis_index("sp")
     tp = lax.axis_index("tp")
@@ -186,6 +212,13 @@
         pltpu.make_async_copy(wo, oall.at[me, pl.ds(0, 128)], lsem.at[6]),
         pltpu.make_async_copy(do, oall.at[me, pl.ds(128, 128)], lsem.at[7]),
     ]
+    small = [
+        pltpu.make_async_copy(src, dst, lsem.at[12 + i])
+        for i, (src, dst) in enumerate(
+            [(gain_h, gain), (freq_h, freq)]
+            + [(g, gains.at[j]) for j, g in enumerate((wqg_h, wkg_h, dqg_h, dkg_h))]
+        )
+    ]
     for c in loads:
         c.start()
     quarter = length // 4
@@ -195,7 +228,7 @@
         )
         for i in range(4)
     ]
-    for c in token_loads:
+    for c in token_loads + small:
         c.start()
     for c in loads[:4]:
         c.wait()
@@ -207,9 +240,11 @@
     pl.semaphore_wait(barrier, 6)
 
     in_ring = PairRing(me, n_sp, wall, depth * 5 // 16, side, other, in_s, in_r, in_ys, in_yr)
-    out_ring = PairRing(me, n_sp, oall, 80, side, other, out_s, out_r, out_ys, out_yr)
-    kv_ring = Ring(me, n_sp, lambda w, p: (kp, vt)[p].at[w], kv_s, kv_r)
+    out_ring = PairRing(me, n_sp, oall, 128, side, other, out_s, in_r, out_ys, out_yr)
+    kv_ring = Ring(me, n_sp, 2, lambda w, p: (kp, vt)[p].at[w], kv_snd, in_r)
     in_ring.begin()
+    for c in small:
+        c.wait()
 
     def norm(i):
         token_loads[i].wait()
@@ -261,7 +296,8 @@
         return carry
 
     def in_step(d, carry):
-        in_ring.hop(d)
+        in_ring.hop_piece(d, 0)
+        in_ring.hop_piece(d, 1)
 
         @pl.when(d == 1)
         def _():
@@ -280,21 +316,23 @@
 
         @pl.when(d >= 4)
         def _():
-            lax.fori_loop(
-                jnp.where(d < 6, 2 * d - 7, d - 1), jnp.where(d < 6, 2 * d - 5, d), projects, 0
-            )
-
+            lax.fori_loop(jnp.where(d == 4, 1, d - 2), d - 1, projects, 0)
+
+        in_ring.hop_piece(d, 2)
+        in_ring.hop_piece(d, 3)
         return carry
 
     lax.fori_loop(1, half, in_step, 0)
     out_ring.begin()
-    in_ring.last()
+    projects(half - 2, 0)
+    in_ring.last_first()
     projects(half - 1, 0)
+    in_ring.last_second()
     in_ring.take_last()
     project(in_ring.owner(0, half))
 
-    def two(ref):
-        return jnp.concatenate([ref[...], ref[...]], axis=1)
+    def two(which):
+        return jnp.concatenate([gains[which], gains[which]], axis=1)
 
     def heads(values, g, which, reach, rows):
         squares = values * values
@@ -310,7 +348,7 @@
         return normed * table[which, rows] + turned * table[which + 1, rows]
 
     blocks = [slice(i * 128, i * 128 + 128) for i in range(length // 128)]
-    g = two(dkg)
+    g = two(3)
     keys = [
         heads(acc[rows, 384:512], g, 2, HD // 4, rows)
         for rows in (slice(0, half_rows), slice(half_rows, length))
@@ -318,7 +356,7 @@
     kp[me] = jnp.where(low_lane, keys[0], pltpu.roll(keys[1], HD, 1)).astype(BF16)
     for rows in blocks:
         vt[me, :, rows] = acc[rows, 384:512].T[HD:].astype(BF16)
-    g = two(wkg)
+    g = two(1)
     for i, rows in enumerate(blocks):
         values = acc[rows, 128:256]
         kvw[pl.ds(WINDOW + i * 128, 128)] = jnp.where(
@@ -340,7 +378,7 @@
     for c in halos:
         c.start()
     scale = HD ** (-0.5)
-    g = two(dqg)
+    g = two(2)
     for rows in blocks:
         q = heads(acc[rows, 256:384], g, 2, HD // 4, rows) * (scale * math.log2(math.e))
         q = q.T.astype(BF16)
@@ -349,7 +387,7 @@
                 cols_h = slice(h * length + rows.start, h * length + rows.stop)
                 qd[p, p * HD : p * HD + HD, cols_h] = q[h * HD : h * HD + HD]
                 qd[p, (1 - p) * HD : (1 - p) * HD + HD, cols_h] = jnp.zeros((HD, 128), BF16)
-    g = two(wqg)
+    g = two(0)
     for rows in blocks:
         q = heads(acc[rows, 0:128], g, 0, HD // 2, rows).astype(BF16).astype(F32) * scale
         qw[0, rows] = jnp.where(low_lane, q, 0.0).astype(BF16)
@@ -409,19 +447,24 @@
     def kv_step(d, carry):
         @pl.when(d < half)
         def _():
-            kv_ring.hop(d)
-
-        @pl.when((d <= OUT_EARLY) & (d < half))
-        def _():
-            out_ring.hop(d)
-
-        @pl.when((d == OUT_EARLY) & (d == half))
+            kv_ring.hop_piece(d, 0)
+            kv_ring.hop_piece(d, 1)
+
+        @pl.when((d + 1 < half))
+        def _():
+            out_ring.hop_piece(d + 1, 0)
+
+        @pl.when(d >= 2)
+        def _():
+            dense((kv_ring.owner(0, d - 1), kv_ring.owner(1, d - 1)))
+
+        @pl.when((d + 1 < half))
+        def _():
+            out_ring.hop_piece(d + 1, 1)
+
+        @pl.when((d + 1 == half))
         def _():
             out_ring.last()
-
-        @pl.when(d >= 2)
-        def _():
-            dense((kv_ring.owner(0, d - 1), kv_ring.owner(1, d - 1)))
 
         @pl.when(d == 3)
         def _():
@@ -434,6 +477,8 @@
 
         return carry
 
+    for p in range(2):
+        out_ring.hop_piece(1, p)
     lax.fori_loop(1, half + 1, kv_step, 0)
     kv_ring.last()
     dense((me, kv_ring.owner(0, half)))
@@ -464,28 +509,33 @@
     ways = ((x_up, up, x_down, down), (x_down, down, x_up, up))
 
     def pair_copy(s):
-        return remote(dsend.at[s], drecv.at[s], d_s.at[s], d_r.at[s], partner)
+        return remote(dsend.at[s], drecv.at[s], d_s.at[lax.rem(s, 2)], d_r.at[s], partner)
 
     def far_copy(s, b):
-        return remote(xs.at[s, b, far], r2.at[s, b], x_s.at[0, s, b], x_r.at[0, s, b], ways[b][0])
+        return remote(xs.at[s, b, far], r2.at[s, b], x_s.at[0, lax.rem(s, 4), b], x_r.at[0, s, b], ways[b][0])
 
     def chain_copy(s, b):
-        return remote(c1.at[s, b], rc.at[s, b], x_s.at[1, s, b], x_r.at[1, s, b], ways[b][0])
+        return remote(c1.at[s, b], rc.at[s, b], x_s.at[1, lax.rem(s, 4), b], x_r.at[1, s, b], ways[b][0])
 
     def near_copy(s, b):
         return remote(
-            xs.at[s, b, ways[b][3]], rd.at[s, b], x_s.at[2, s, b], x_r.at[2, s, b], ways[b][2]
+            xs.at[s, b, ways[b][3]], rd.at[s, b], x_s.at[2, lax.rem(s, 4), b], x_r.at[2, s, b], ways[b][2]
         )
 
     def put(s, b):
         at = pl.multiple_of(owners_of(s)[b] * cols, cols)
-        return pltpu.make_async_copy(held.at[s - 1, b], out.at[:, pl.ds(at, cols)], o_s.at[s - 1, b])
+        return pltpu.make_async_copy(held.at[s - 1, b], out.at[:, pl.ds(at, cols)], o_s.at[lax.rem(s, 2), b])
 
     def stage1(s):
         owners = owners_of(s)
         for b in range(2):
             dsend[s - 1, b] = nn(att[pl.ds(theirs_at, half_rows)], oall[owners[b]]).astype(BF16)
         mine[s - 1, 0] = nn(att[pl.ds(mine_at, half_rows)], oall[owners[0]])
+
+        @pl.when(s > 2)
+        def _():
+            pair_copy(s - 3).wait_send()
+
         pair_copy(s - 1).start()
         mine[s - 1, 1] = nn(att[pl.ds(mine_at, half_rows)], oall[owners[1]])
 
@@ -495,10 +545,14 @@
             both = (mine[s - 1, b] + drecv[s - 1, b].astype(F32)).astype(BF16)
             for t in range(n_x):
                 xs[s - 1, b, t] = both[t * share : t * share + share]
+
+        @pl.when(s > 4)
+        def _():
+            for b in range(2):
+                far_copy(s - 5, b).wait_send()
+
         for b in range(2):
             far_copy(s - 1, b).start()
-        for b in range(2):
-            near_copy(s - 1, b).start()
 
     def stage3(s):
         for b in range(2):
@@ -506,8 +560,23 @@
             c1[s - 1, b] = (xs[s - 1, b, ways[b][1]].astype(F32) + r2[s - 1, b].astype(F32)).astype(
                 BF16
             )
+
+        @pl.when(s > 4)
+        def _():
+            for b in range(2):
+                chain_copy(s - 5, b).wait_send()
+
         for b in range(2):
             chain_copy(s - 1, b).start()
+
+    def send_near(s):
+        @pl.when(s > 4)
+        def _():
+            for b in range(2):
+                near_copy(s - 5, b).wait_send()
+
+        for b in range(2):
+            near_copy(s - 1, b).start()
 
     def stage4(s):
         for b in range(2):
@@ -517,20 +586,16 @@
                 xs[s - 1, b, xc].astype(F32) + rc[s - 1, b].astype(F32) + rd[s - 1, b].astype(F32)
             )
             held[s - 1, b] = total.astype(BF16)
+
+        @pl.when(s > 2)
+        def _():
+            for b in range(2):
+                put(s - 2, b).wait()
+
         for b in range(2):
             put(s, b).start()
 
     def out_step(s, carry):
-        ahead = s + OUT_EARLY
-
-        @pl.when(ahead < half)
-        def _():
-            out_ring.hop(ahead)
-
-        @pl.when(ahead == half)
-        def _():
-            out_ring.last()
-
         @pl.when(s < half)
         def _():
             out_ring.take(s)
@@ -551,9 +616,13 @@
         def _():
             stage3(s - LAG[1])
 
-        @pl.when(s >= 1 + LAG[2])
-        def _():
-            stage4(s - LAG[2])
+        @pl.when((s >= 1 + LAG[2]) & (s <= half + LAG[2]))
+        def _():
+            send_near(s - LAG[2])
+
+        @pl.when(s >= 1 + LAG[3])
+        def _():
+            stage4(s - LAG[3])
 
         @pl.when(s == 3)
         def _():
@@ -564,20 +633,22 @@
 
         return carry
 
-    lax.fori_loop(1, half + LAG[2] + 1, out_step, 0)
+    lax.fori_loop(1, half + LAG[3] + 1, out_step, 0)
 
     out_ring.drain()
 
     def drain(s, carry):
-        pair_copy(s).wait_send()
         for b in range(2):
             far_copy(s, b).wait_send()
             near_copy(s, b).wait_send()
             chain_copy(s, b).wait_send()
+        return carry
+
+    lax.fori_loop(half - 4, half, drain, 0)
+    for s in (half - 2, half - 1):
+        pair_copy(s).wait_send()
+        for b in range(2):
             put(s + 1, b).wait()
-        return carry
-
-    lax.fori_loop(0, half, drain, 0)
 
 
 def frequencies():
@@ -597,13 +668,13 @@
         half, n_x, share = n_sp // 2, n_tp // 2, length // n_tp
         assert wq.shape[1] == dq.shape[1] == 2 * HD and wk.shape[1] == dk.shape[1] == HD
         assert length % 128 == 0 and share % 16 == 0 and width == depth * n_sp
-        any_, vmem = pl.BlockSpec(memory_space=pl.ANY), pl.BlockSpec(memory_space=pltpu.VMEM)
+        any_ = pl.BlockSpec(memory_space=pl.ANY)
         smem = pl.BlockSpec(memory_space=pltpu.SMEM)
         dma = pltpu.SemaphoreType.DMA
         return pl.pallas_call(
             functools.partial(kernel, n_sp, n_tp),
             out_shape=jax.ShapeDtypeStruct((share, cols * n_sp), BF16),
-            in_specs=[any_, vmem, any_, any_, any_, vmem, vmem, smem, any_, any_, any_, vmem, vmem, any_, any_, vmem],
+            in_specs=[any_] * 7 + [smem] + [any_] * 8,
             out_specs=any_,
             scratch_shapes=[
                 pltpu.VMEM((length, width), BF16),
@@ -629,25 +700,26 @@
                 pltpu.VMEM((half, 2, share, cols), BF16),
                 pltpu.VMEM((half, 2, share, cols), BF16),
                 pltpu.VMEM((half, 2, share, cols), BF16),
-                dma((12,)),
-                dma((2, half, 2)),
-                dma((2, half, 2)),
-                dma((2, half, 2)),
-                dma((2, half, 2)),
-                dma((2, half, 2)),
-                dma((2, half, 2)),
+                dma((18,)),
+                dma((2, 2, 4)),
+                dma((2, half, 4)),
+                dma((2, 2, 2)),
+                dma((2,)),
                 dma((2,)),
                 dma((2,)),
                 dma((half,)),
-                dma((half,)),
+                dma((3, 4, 2)),
                 dma((3, half, 2)),
-                dma((3, half, 2)),
+                dma((2, 2)),
                 dma((2, half)),
-                dma((2, half)),
-                dma((2, half)),
+                dma((2, 2)),
                 dma((2, half)),
                 pltpu.VMEM((half, 2, share, cols), BF16),
-                dma((half, 2)),
+                dma((2, 2)),
+                pltpu.VMEM((width // 128, 128), F32),
+                pltpu.VMEM((4, 1, HD), F32),
+                pltpu.VMEM((2, 128), F32),
+                dma((2, 2, 2)),
             ],
             compiler_params=pltpu.CompilerParams(
                 collective_id=0, has_side_effects=True, vmem_limit_bytes=60 * 1024 * 1024

time: 124 us -> 116 us (0.935)
  Pallas kernels: 122 us -> 114 us
    pallas_call x1, Pallas kernels: 122 us -> 114 us  [local(): pl.pallas_call(functools.partial(kernel, n_sp, n_tp), out_shape=jax.Shape...]
where the time goes in v3:
time: 116 us
  Pallas kernels  114 us (98%)
  local copies, waits for them, and re-layouts  1.77 us (2%)
    pallas_call x1, Pallas kernels, local(): pl.pallas_call(functools.partial(kernel, n_sp, n_tp), out_shape=jax.Shape...  114 us

profile of v3, /device:TPU:33, one launch (start us, length us, event | category | flops | bytes accessed | tf_op | source)
XLA Modules:
  0.0 115.6 jit_solution(12238357112160883999)
XLA Ops:
  0.0 113.8 %shard_map.154 = bf16[48,4096]{1,0:T(8,128)(2,1)} custom-call(bf16[384,4096]{1,0:T(8,128)(2,1)} %tokens.1, f32[32,128]{1,0:T(8,128)} %bitcast.13, bf16[256,128]{1,0:T(8,128)(2,1)} %wq.1, bf16[64,256]{1,0:T(8,128)(2,1)} %bitcast.9, bf16[64,256]{1,0:T(8,128)(2,1)} %bitcast.10, f32[1,64]{1,0:T(1,128)} %bitcast.14, f32[1,64]{1,0:T(1,128)} %bitcast.15, f32[2]{0:T(128)} %sink.1, ...), custom_call_target="tpu_custom_call" | custom-call | tf_op jit(solution)/shard_map/pallas_call | solution.py:674
  113.8 1.8 %copy.18 = bf16[48,4096]{1,0:T(8,128)(2,1)} copy(bf16[48,4096]{1,0:T(8,128)(2,1)} %shard_map.154) | data formatting | bytes 786432

commit v4 on v3

--- a/solution.py
+++ b/solution.py
@@ -19,6 +19,7 @@
 BF16 = jnp.bfloat16
 LOW = -1e30
 LAG = (1, 5, 2, 13)
+EARLY = 1
 
 
 def nt(a, b):
@@ -36,8 +37,7 @@
 
 
 class Ring:
-    def __init__(self, me, n, count, piece, send_sem, recv_sem, place=0):
-        self.place = place
+    def __init__(self, me, n, count, piece, send_sem, recv_sem):
         self.me, self.n, self.half = me, n, n // 2
         self.count = count
         self.piece, self.send_sem, self.recv_sem = piece, send_sem, recv_sem
@@ -50,7 +50,7 @@
     def copy(self, way, step, p, distance):
         ref = self.piece(self.owner(way, distance), p)
         return remote(
-            ref, ref, self.send_sem.at[way, lax.rem(step, 2), p], self.recv_sem.at[way, step, self.place + p], self.to[way]
+            ref, ref, self.send_sem.at[way, lax.rem(step, 2), p], self.recv_sem.at[way, step, p], self.to[way]
         )
 
     def send(self, way, step, p):
@@ -66,8 +66,8 @@
     def way_of(self, p):
         return 2 * p // self.count
 
-    def begin(self):
-        for p in range(self.count):
+    def begin(self, pieces=None):
+        for p in pieces or range(self.count):
             for way in range(2):
                 self.copy(way, 0, p, 0).start()
 
@@ -119,7 +119,7 @@
                 return ref.at[w, pl.ds(at, cuts[p][1])]
             return ref.at[w, pl.ds(*later[p - 2])]
 
-        super().__init__(me, n, 2 + len(later), piece, send_sem, recv_sem, 0 if later else 2)
+        super().__init__(me, n, 2 + len(later), piece, send_sem, recv_sem)
 
     def across(self, way, step, at):
         ref = self.ref.at[self.owner(way, step), pl.ds(at, self.give)]
@@ -160,8 +160,7 @@
     def take_last(self):
         self.across(0, self.half, self.taken_at).wait_recv()
 
-    def drain(self):
-        super().drain()
+    def drain_pair(self):
         self.across(0, self.half, self.given_at).wait_send()
         for way in range(2):
             self.across(way, self.half - 1, self.given_at).wait_send()
@@ -174,8 +173,8 @@
     out,
     x, wall, stage, acc, oall, kp, vt, kvw, qd, qw, att, attw, m_s, a_s,
     table, dsend, drecv, mine, xs, r2, c1, rc, rd,
-    lsem, in_s, in_r, out_s, halo_s, halo_r,
-    d_s, d_r, x_s, x_r, in_ys, in_yr, out_ys, out_yr, held, o_s,
+    in_s, in_r, out_s, out_r, halo_s, halo_r,
+    d_s, d_r, x_r, in_ys, in_yr, out_ys, out_yr, held, o_s,
     gain, gains, freq, kv_snd,
 ):
     me = lax.axis_index("sp")
@@ -202,18 +201,20 @@
     for peer in (right, left, partner, x_up, x_down, other):
         pl.semaphore_signal(barrier, inc=1, device_id=peer, device_id_type=MESH)
 
+    load_sems = [kv_snd.at[i // 8, i // 4 % 2, i % 4] for i in range(16)]
+    load_sems += [halo_s.at[i] for i in range(2)]
     loads = [
-        pltpu.make_async_copy(wk, stage.at[0], lsem.at[0]),
-        pltpu.make_async_copy(wv, stage.at[1], lsem.at[1]),
-        pltpu.make_async_copy(dk, stage.at[2], lsem.at[2]),
-        pltpu.make_async_copy(dv, stage.at[3], lsem.at[3]),
-        pltpu.make_async_copy(wq, wall.at[me, :, pl.ds(0, 128)], lsem.at[4]),
-        pltpu.make_async_copy(dq, wall.at[me, :, pl.ds(256, 128)], lsem.at[5]),
-        pltpu.make_async_copy(wo, oall.at[me, pl.ds(0, 128)], lsem.at[6]),
-        pltpu.make_async_copy(do, oall.at[me, pl.ds(128, 128)], lsem.at[7]),
+        pltpu.make_async_copy(wk, stage.at[0], load_sems[0]),
+        pltpu.make_async_copy(wv, stage.at[1], load_sems[1]),
+        pltpu.make_async_copy(dk, stage.at[2], load_sems[2]),
+        pltpu.make_async_copy(dv, stage.at[3], load_sems[3]),
+        pltpu.make_async_copy(wq, wall.at[me, :, pl.ds(0, 128)], load_sems[4]),
+        pltpu.make_async_copy(dq, wall.at[me, :, pl.ds(256, 128)], load_sems[5]),
+        pltpu.make_async_copy(wo, oall.at[me, pl.ds(0, 128)], load_sems[6]),
+        pltpu.make_async_copy(do, oall.at[me, pl.ds(128, 128)], load_sems[7]),
     ]
     small = [
-        pltpu.make_async_copy(src, dst, lsem.at[12 + i])
+        pltpu.make_async_copy(src, dst, load_sems[12 + i])
         for i, (src, dst) in enumerate(
             [(gain_h, gain), (freq_h, freq)]
             + [(g, gains.at[j]) for j, g in enumerate((wqg_h, wkg_h, dqg_h, dkg_h))]
@@ -224,7 +225,7 @@
     quarter = length // 4
     token_loads = [
         pltpu.make_async_copy(
-            tokens.at[pl.ds(i * quarter, quarter)], x.at[pl.ds(i * quarter, quarter)], lsem.at[8 + i]
+            tokens.at[pl.ds(i * quarter, quarter)], x.at[pl.ds(i * quarter, quarter)], load_sems[8 + i]
         )
         for i in range(4)
     ]
@@ -239,9 +240,14 @@
         c.wait()
     pl.semaphore_wait(barrier, 6)
 
+    pair_rows = (kp.shape[1] // 2, vt.shape[1] // 2)
     in_ring = PairRing(me, n_sp, wall, depth * 5 // 16, side, other, in_s, in_r, in_ys, in_yr)
-    out_ring = PairRing(me, n_sp, oall, 128, side, other, out_s, in_r, out_ys, out_yr)
-    kv_ring = Ring(me, n_sp, 2, lambda w, p: (kp, vt)[p].at[w], kv_snd, in_r)
+    out_ring = PairRing(me, n_sp, oall, 128, side, other, out_s, out_r, out_ys, out_yr)
+    kv_ring = Ring(
+        me, n_sp, 4,
+        lambda w, p: (kp, vt)[p // 2].at[w, pl.ds(p % 2 * (pair_rows[p // 2]), pair_rows[p // 2])],
+        kv_snd, in_r,
+    )
     in_ring.begin()
     for c in small:
         c.wait()
@@ -328,6 +334,8 @@
     in_ring.last_first()
     projects(half - 1, 0)
     in_ring.last_second()
+    for p in range(2):
+        out_ring.hop_piece(1, p)
     in_ring.take_last()
     project(in_ring.owner(0, half))
 
@@ -356,13 +364,14 @@
     kp[me] = jnp.where(low_lane, keys[0], pltpu.roll(keys[1], HD, 1)).astype(BF16)
     for rows in blocks:
         vt[me, :, rows] = acc[rows, 384:512].T[HD:].astype(BF16)
+    kv_ring.begin((0, 1))
     g = two(1)
     for i, rows in enumerate(blocks):
         values = acc[rows, 128:256]
         kvw[pl.ds(WINDOW + i * 128, 128)] = jnp.where(
             low_lane, heads(values, g, 0, HD // 2, rows), values
         ).astype(BF16)
-    kv_ring.begin()
+    kv_ring.begin((2, 3))
     halos = [
         remote(
             kvw.at[pl.ds(length, WINDOW)], kvw.at[pl.ds(0, WINDOW)], halo_s.at[0], halo_r.at[0], right
@@ -427,13 +436,13 @@
 
     ones = jnp.ones((8, 2 * length), BF16)
 
-    def dense(owners):
+    def dense(owners, cut=slice(None)):
         keys = jnp.concatenate([kp[w] for w in owners], axis=0)
         values = jnp.concatenate(
             [jnp.concatenate([vt[w] for w in owners], axis=1), ones], axis=0
         )
-        low, high = nn(keys, qd[0]), nn(keys, qd[1])
-        before = m_s[...]
+        low, high = nn(keys, qd[0, :, cut]), nn(keys, qd[1, :, cut])
+        before = m_s[:, cut]
         top = jnp.maximum(before, jnp.max(jnp.maximum(low, high), axis=0, keepdims=True))
         shrink = jnp.exp2(before - top)
         low = jnp.exp2(low - top[:1]).astype(BF16)
@@ -441,44 +450,50 @@
         expons = jnp.concatenate(
             [low[:half_rows], high[:half_rows], low[half_rows:], high[half_rows:]], axis=0
         )
-        a_s[...] = a_s[...] * shrink[:1] + nn(values, expons)
-        m_s[...] = top
+        a_s[:, cut] = a_s[:, cut] * shrink[:1] + nn(values, expons)
+        m_s[:, cut] = top
 
     def kv_step(d, carry):
-        @pl.when(d < half)
-        def _():
-            kv_ring.hop_piece(d, 0)
-            kv_ring.hop_piece(d, 1)
-
-        @pl.when((d + 1 < half))
-        def _():
-            out_ring.hop_piece(d + 1, 0)
-
-        @pl.when(d >= 2)
-        def _():
-            dense((kv_ring.owner(0, d - 1), kv_ring.owner(1, d - 1)))
-
-        @pl.when((d + 1 < half))
-        def _():
-            out_ring.hop_piece(d + 1, 1)
-
-        @pl.when((d + 1 == half))
+        for h in range(2):
+
+            @pl.when(d < half)
+            def _():
+                kv_ring.hop_piece(d, 2 * h)
+                kv_ring.hop_piece(d, 2 * h + 1)
+
+            @pl.when(d >= 2)
+            def _():
+                dense(
+                    (kv_ring.owner(0, d - 1), kv_ring.owner(1, d - 1)),
+                    slice(h * length, h * length + length),
+                )
+
+        @pl.when(d + EARLY < half)
+        def _():
+            out_ring.hop_piece(d + EARLY, 0)
+
+        @pl.when((d >= 3) & (d < 3 + length // 128))
+        def _():
+            window(d - 3)
+
+        @pl.when(d + EARLY < half)
+        def _():
+            out_ring.hop_piece(d + EARLY, 1)
+
+        @pl.when(d + EARLY == half)
         def _():
             out_ring.last()
 
-        @pl.when(d == 3)
+        @pl.when(d == 2)
         def _():
             for c in halos:
                 c.wait_recv()
 
-        @pl.when((d >= 3) & (d < 3 + length // 128))
-        def _():
-            window(d - 3)
-
         return carry
 
-    for p in range(2):
-        out_ring.hop_piece(1, p)
+    for h in range(2, EARLY + 1):
+        for p in range(2):
+            out_ring.hop_piece(h, p)
     lax.fori_loop(1, half + 1, kv_step, 0)
     kv_ring.last()
     dense((me, kv_ring.owner(0, half)))
@@ -512,14 +527,14 @@
         return remote(dsend.at[s], drecv.at[s], d_s.at[lax.rem(s, 2)], d_r.at[s], partner)
 
     def far_copy(s, b):
-        return remote(xs.at[s, b, far], r2.at[s, b], x_s.at[0, lax.rem(s, 4), b], x_r.at[0, s, b], ways[b][0])
+        return remote(xs.at[s, b, far], r2.at[s, b], in_s.at[0, b, lax.rem(s, 4)], x_r.at[0, s, b], ways[b][0])
 
     def chain_copy(s, b):
-        return remote(c1.at[s, b], rc.at[s, b], x_s.at[1, lax.rem(s, 4), b], x_r.at[1, s, b], ways[b][0])
+        return remote(c1.at[s, b], rc.at[s, b], in_s.at[1, b, lax.rem(s, 4)], x_r.at[1, s, b], ways[b][0])
 
     def near_copy(s, b):
         return remote(
-            xs.at[s, b, ways[b][3]], rd.at[s, b], x_s.at[2, lax.rem(s, 4), b], x_r.at[2, s, b], ways[b][2]
+            xs.at[s, b, ways[b][3]], rd.at[s, b], out_s.at[b, lax.div(lax.rem(s, 4), 2), lax.rem(s, 2)], x_r.at[2, s, b], ways[b][2]
         )
 
     def put(s, b):
@@ -626,16 +641,18 @@
 
         @pl.when(s == 3)
         def _():
-            in_ring.drain()
+            in_ring.drain_pair()
             kv_ring.drain()
             for c in halos:
                 c.wait_send()
 
         return carry
 
+    in_ring.drain()
+    out_ring.drain()
     lax.fori_loop(1, half + LAG[3] + 1, out_step, 0)
 
-    out_ring.drain()
+    out_ring.drain_pair()
 
     def drain(s, carry):
         for b in range(2):
@@ -700,15 +717,14 @@
                 pltpu.VMEM((half, 2, share, cols), BF16),
                 pltpu.VMEM((half, 2, share, cols), BF16),
                 pltpu.VMEM((half, 2, share, cols), BF16),
-                dma((18,)),
                 dma((2, 2, 4)),
                 dma((2, half, 4)),
                 dma((2, 2, 2)),
+                dma((2, half, 2)),
                 dma((2,)),
                 dma((2,)),
                 dma((2,)),
                 dma((half,)),
-                dma((3, 4, 2)),
                 dma((3, half, 2)),
                 dma((2, 2)),
                 dma((2, half)),
@@ -719,7 +735,7 @@
                 pltpu.VMEM((width // 128, 128), F32),
                 pltpu.VMEM((4, 1, HD), F32),
                 pltpu.VMEM((2, 128), F32),
-                dma((2, 2, 2)),
+                dma((2, 2, 4)),
             ],
             compiler_params=pltpu.CompilerParams(
                 collective_id=0, has_side_effects=True, vmem_limit_bytes=60 * 1024 * 1024

time: 116 us -> 115 us (level)
  no operation moved by 1% of the time
where the time goes in v4:
time: 115 us
  Pallas kernels  113 us (98%)
  local copies, waits for them, and re-layouts  1.77 us (2%)
    pallas_call x1, Pallas kernels, local(): pl.pallas_call(functools.partial(kernel, n_sp, n_tp), out_shape=jax.Shape...  113 us

profile of v4, /device:TPU:33, one launch (start us, length us, event | category | flops | bytes accessed | tf_op | source)
XLA Modules:
  0.0 114.6 jit_solution(16010409636760314640)
XLA Ops:
  0.0 112.8 %shard_map.154 = bf16[48,4096]{1,0:T(8,128)(2,1)} custom-call(bf16[384,4096]{1,0:T(8,128)(2,1)} %tokens.1, f32[32,128]{1,0:T(8,128)} %bitcast.13, bf16[256,128]{1,0:T(8,128)(2,1)} %wq.1, bf16[64,256]{1,0:T(8,128)(2,1)} %bitcast.9, bf16[64,256]{1,0:T(8,128)(2,1)} %bitcast.10, f32[1,64]{1,0:T(1,128)} %bitcast.14, f32[1,64]{1,0:T(1,128)} %bitcast.15, f32[2]{0:T(128)} %sink.1, ...), custom_call_target="tpu_custom_call" | custom-call | tf_op jit(solution)/shard_map/pallas_call | solution.py:691
  112.8 1.8 %copy.18 = bf16[48,4096]{1,0:T(8,128)(2,1)} copy(bf16[48,4096]{1,0:T(8,128)(2,1)} %shard_map.154) | data formatting | bytes 786432

commit v5 on v4

--- a/solution.py
+++ b/solution.py
@@ -174,8 +174,7 @@
     x, wall, stage, acc, oall, kp, vt, kvw, qd, qw, att, attw, m_s, a_s,
     table, dsend, drecv, mine, xs, r2, c1, rc, rd,
     in_s, in_r, out_s, out_r, halo_s, halo_r,
-    d_s, d_r, x_r, in_ys, in_yr, out_ys, out_yr, held, o_s,
-    gain, gains, freq, kv_snd,
+    d_s, d_r, x_r, in_ys, in_yr, out_ys, out_yr, gain, gains, freq, kv_snd,
 ):
     me = lax.axis_index("sp")
     tp = lax.axis_index("tp")
@@ -537,10 +536,6 @@
             xs.at[s, b, ways[b][3]], rd.at[s, b], out_s.at[b, lax.div(lax.rem(s, 4), 2), lax.rem(s, 2)], x_r.at[2, s, b], ways[b][2]
         )
 
-    def put(s, b):
-        at = pl.multiple_of(owners_of(s)[b] * cols, cols)
-        return pltpu.make_async_copy(held.at[s - 1, b], out.at[:, pl.ds(at, cols)], o_s.at[lax.rem(s, 2), b])
-
     def stage1(s):
         owners = owners_of(s)
         for b in range(2):
@@ -600,15 +595,8 @@
             total = (
                 xs[s - 1, b, xc].astype(F32) + rc[s - 1, b].astype(F32) + rd[s - 1, b].astype(F32)
             )
-            held[s - 1, b] = total.astype(BF16)
-
-        @pl.when(s > 2)
-        def _():
-            for b in range(2):
-                put(s - 2, b).wait()
-
-        for b in range(2):
-            put(s, b).start()
+            at = pl.multiple_of(owners_of(s)[b] * cols, cols)
+            out[:, pl.ds(at, cols)] = total.astype(BF16)
 
     def out_step(s, carry):
         @pl.when(s < half)
@@ -664,8 +652,6 @@
     lax.fori_loop(half - 4, half, drain, 0)
     for s in (half - 2, half - 1):
         pair_copy(s).wait_send()
-        for b in range(2):
-            put(s + 1, b).wait()
 
 
 def frequencies():
@@ -690,9 +676,9 @@
         dma = pltpu.SemaphoreType.DMA
         return pl.pallas_call(
             functools.partial(kernel, n_sp, n_tp),
-            out_shape=jax.ShapeDtypeStruct((share, cols * n_sp), BF16),
+            out_shape=pltpu.VMEM((share, cols * n_sp), BF16),
             in_specs=[any_] * 7 + [smem] + [any_] * 8,
-            out_specs=any_,
+            out_specs=pl.BlockSpec(memory_space=pltpu.VMEM),
             scratch_shapes=[
                 pltpu.VMEM((length, width), BF16),
                 pltpu.VMEM((n_sp, depth, 512), BF16),
@@ -730,8 +716,6 @@
                 dma((2, half)),
                 dma((2, 2)),
                 dma((2, half)),
-                pltpu.VMEM((half, 2, share, cols), BF16),
-                dma((2, 2)),
                 pltpu.VMEM((width // 128, 128), F32),
                 pltpu.VMEM((4, 1, HD), F32),
                 pltpu.VMEM((2, 128), F32),

time: 115 us -> 113 us (0.983)
  no operation moved by 1% of the time
where the time goes in v5:
time: 113 us
  Pallas kernels  112 us (99%)
    pallas_call x1, Pallas kernels, local(): pl.pallas_call(functools.partial(kernel, n_sp, n_tp), out_shape=pltpu.VME...  112 us

profile of v5, /device:TPU:33, one launch (start us, length us, event | category | flops | bytes accessed | tf_op | source)
XLA Modules:
  0.0 113.0 jit_solution(15606612551069529416)
XLA Ops:
  0.0 112.2 %shard_map.154 = bf16[48,4096]{1,0:T(8,128)(2,1)S(1)} custom-call(bf16[384,4096]{1,0:T(8,128)(2,1)} %tokens.1, f32[32,128]{1,0:T(8,128)} %bitcast.13, bf16[256,128]{1,0:T(8,128)(2,1)} %wq.1, bf16[64,256]{1,0:T(8,128)(2,1)} %bitcast.9, bf16[64,256]{1,0:T(8,128)(2,1)} %bitcast.10, f32[1,64]{1,0:T(1,128)} %bitcast.14, f32[1,64]{1,0:T(1,128)} %bitcast.15, ...), custom_call_target="tpu_custom_call" | custom-call | tf_op jit(solution)/shard_map/pallas_call | solution.py:677
  112.2 0.7 copy.18
